TPU v7x, 768 devices: a whole 4x8x12 slice. The times are simulated.
768 devices in a mesh: fs: 192 (over z, y, core), tp: 4 (over x).
Axes of the slice: x: 4, y: 8, z: 12, core: 2. Of those that a mesh axis runs over, the one named last changes fastest.
Arguments:
- inputs: bfloat16 [196608, 3072], P('fs'), may hold values from -6 to 6
- query_cot: bfloat16 [196608, 768], P('fs', 'tp'), may hold values from -0.0134887695 to 0.0134887695
- value_cot: bfloat16 [196608, 1536], P('fs', 'tp'), may hold values from -0.0134887695 to 0.0134887695
- query_factor: bfloat16 [3072, 192], P('fs'), may hold values from -0.109375 to 0.109375
- value_factor: bfloat16 [3072, 192], P('fs'), may hold values from -0.109375 to 0.109375
- query_weight: float32 [3072, 768], P('fs', 'tp'), may hold values from -0.109375 to 0.109375
- value_weight: float32 [3072, 1536], P('fs', 'tp'), may hold values from -0.109375 to 0.109375
- query_first: float32 [192, 768], P('fs', 'tp'), may hold values from -1.6 to 1.6
- query_second: float32 [192, 768], P('fs', 'tp'), may hold values from 0.002 to 0.05
- value_first: float32 [192, 1536], P('fs', 'tp'), may hold values from -1.6 to 1.6
- value_second: float32 [192, 1536], P('fs', 'tp'), may hold values from 0.002 to 0.05
Outputs:
- step_q: float32 [3072, 768], P('fs', 'tp')
- step_v: float32 [3072, 1536], P('fs', 'tp')
- new_q: float32 [3072, 768], P('fs', 'tp')
- new_v: float32 [3072, 1536], P('fs', 'tp')
- first_q: float32 [192, 768], P('fs', 'tp')
- second_q: float32 [192, 768], P('fs', 'tp')
- first_v: float32 [192, 1536], P('fs', 'tp')
- second_v: float32 [192, 1536], P('fs', 'tp')
- copy_q: bfloat16 [3072, 768], P(None, 'tp')
- copy_v: bfloat16 [3072, 1536], P(None, 'tp')
All inputs are finite; a program needn't handle non-finite values.
Results may differ from a plain program's by a relative error of at most 0.0041.
Values may be sent and summed in bfloat16 or wider, within the bound.
No kernel may reach another device: no remote copies, remote signals or barrier semaphores. Data moves between devices by JAX's collectives and lax.ppermute only.
A program may use at most 64 MiB of HBM per device.

v0:
```python
import jax
import jax.numpy as jnp
from jax import lax
from jax.sharding import Mesh
from jax.sharding import PartitionSpec as P

FS = ("fs_0", "fs_1", "fs_2")


first_decay = 0.9
second_decay = 0.99
small_eps = 1e-08
learn_rate = 0.01


def in_one_piece(arrays, axis, dim, along):
    ends, at = ([], 0)
    for a in arrays[:-1]:
        at += a.shape[along]
        ends.append(at)
    both = jnp.concatenate(arrays, axis=along)
    return tuple(jnp.split(lax.all_gather(both, axis, axis=dim, tiled=True), ends, axis=along))


def rows_first(arrays, axis, dims):
    turned = [jnp.moveaxis(a, dim, 0) for a, dim in zip(arrays, dims)]
    widths = [t[0].size for t in turned]
    both = jnp.concatenate([t.reshape(-1, w) for t, w in zip(turned, widths)], axis=1)
    whole = lax.all_gather(both, axis, axis=0, tiled=True)
    blocks = jnp.split(whole, [sum(widths[:k]) for k in range(1, len(widths))], axis=1)
    return tuple(
        (
            jnp.moveaxis(b.reshape(-1, *t.shape[1:]), 0, dim)
            for b, t, dim in zip(blocks, turned, dims)
        )
    )


def filled_up(lines, size):
    spare = -lines.shape[0] % size
    if not spare:
        return lines
    return jnp.concatenate([lines, jnp.zeros((spare, *lines.shape[1:]), lines.dtype)])


def sum_by_parts(value, near, far):
    lines = value.reshape(-1, *value.shape[1:][-1:])
    padded = filled_up(lines, lax.axis_size(near))
    own = lax.psum_scatter(padded, near, scatter_dimension=0, tiled=True)
    own = lax.psum(own, far)
    whole = lax.all_gather(own, near, axis=0, tiled=True)
    return whole[: len(lines)].reshape(value.shape)


def sent_to_all(value, axis):
    size = lax.axis_size(axis)
    return lax.all_to_all(
        jnp.broadcast_to(value[None], (size, *value.shape)), axis, 0, 0, tiled=True
    )


def taken_together(value, axis):
    return sent_to_all(value, axis).sum(axis=0)


def moments(old_first, old_second, gradient):
    first = first_decay * old_first + (1.0 - first_decay) * gradient
    second = second_decay * old_second + (1.0 - second_decay) * gradient * gradient
    unit = first / (jnp.sqrt(second) + small_eps)
    return (first, second, unit)


def on_device(
    inputs,
    query_cot,
    value_cot,
    query_factor,
    value_factor,
    query_weight,
    value_weight,
    query_first,
    query_second,
    value_first,
    value_second,
):
    rank_cols = query_factor.shape[1]
    q_cols = query_cot.shape[1]
    v_cols = value_cot.shape[1]
    own_rows = query_first.shape[0]
    entries = rank_cols * (q_cols + v_cols) * lax.axis_size("tp")
    piece_width = rank_cols // lax.axis_size("tp")
    col_start = lax.axis_index("tp") * piece_width
    q_piece = lax.dynamic_slice_in_dim(query_factor, col_start, piece_width, 1)
    v_piece = lax.dynamic_slice_in_dim(value_factor, col_start, piece_width, 1)
    pieces = in_one_piece((q_piece, v_piece), FS, 0, 1)
    sum_q = jnp.dot(inputs, pieces[0], preferred_element_type=jnp.float32)
    sum_v = jnp.dot(inputs, pieces[1], preferred_element_type=jnp.float32)
    proj_q = sum_q.astype(jnp.bfloat16)
    proj_v = sum_v.astype(jnp.bfloat16)
    proj_q, proj_v = rows_first((proj_q, proj_v), "tp", (1, 1))
    term_q = lax.dot_general(
        proj_q, query_cot, (((0,), (0,)), ((), ())), preferred_element_type=jnp.float32
    )
    term_v = lax.dot_general(
        proj_v, value_cot, (((0,), (0,)), ((), ())), preferred_element_type=jnp.float32
    )
    full_sums = sum_by_parts(jnp.concatenate([term_q, term_v], axis=1), "fs_2", ("fs_0", "fs_1"))
    stacked = in_one_piece((query_first, query_second, value_first, value_second), FS, 0, 1)
    all_first_q, all_second_q, unit_q = moments(stacked[0], stacked[1], full_sums[:, :q_cols])
    all_first_v, all_second_v, unit_v = moments(stacked[2], stacked[3], full_sums[:, q_cols:])
    norm_total = taken_together(jnp.sum(unit_q * unit_q) + jnp.sum(unit_v * unit_v), "tp")
    step_scale = lax.rsqrt(norm_total / entries + 1e-06)
    whole_q = (step_scale * unit_q).astype(jnp.bfloat16)
    whole_v = (step_scale * unit_v).astype(jnp.bfloat16)
    row_begin = lax.axis_index(FS) * own_rows
    first_q = lax.dynamic_slice_in_dim(all_first_q, row_begin, own_rows, 0)
    second_q = lax.dynamic_slice_in_dim(all_second_q, row_begin, own_rows, 0)
    first_v = lax.dynamic_slice_in_dim(all_first_v, row_begin, own_rows, 0)
    second_v = lax.dynamic_slice_in_dim(all_second_v, row_begin, own_rows, 0)
    step_q = jnp.dot(query_factor, whole_q, preferred_element_type=jnp.float32)
    step_v = jnp.dot(value_factor, whole_v, preferred_element_type=jnp.float32)
    new_q = query_weight - learn_rate * step_q
    new_v = value_weight - learn_rate * step_v
    copy_q, copy_v = in_one_piece(
        (new_q.astype(jnp.bfloat16), new_v.astype(jnp.bfloat16)), FS, 0, 1
    )
    return (step_q, step_v, new_q, new_v, first_q, second_q, first_v, second_v, copy_q, copy_v)


def solution(mesh):
    split = Mesh(mesh.devices.reshape(12, 8, 2, mesh.shape["tp"]), ("fs_0", "fs_1", "fs_2", "tp"))
    return jax.shard_map(
        on_device,
        mesh=split,
        in_specs=(
            P(FS, None),
            P(FS, "tp"),
            P(FS, "tp"),
            P(FS, None),
            P(FS, None),
            P(FS, "tp"),
            P(FS, "tp"),
            P(FS, "tp"),
            P(FS, "tp"),
            P(FS, "tp"),
            P(FS, "tp"),
        ),
        out_specs=(
            P(FS, "tp"),
            P(FS, "tp"),
            P(FS, "tp"),
            P(FS, "tp"),
            P(FS, "tp"),
            P(FS, "tp"),
            P(FS, "tp"),
            P(FS, "tp"),
            P(None, "tp"),
            P(None, "tp"),
        ),
        check_vma=False,
    )
```

profile of v0, /device:TPU:1, one launch (start us, length us, event | category | flops | bytes accessed | tf_op | source)
XLA Modules:
  0.0 508.4 jit_solution(14217817907343546589)
XLA Ops:
  7.2 0.0 copy-start
  7.2 0.0 reduce-scatter.2.cloned.1.call-start
  7.2 0.0 copy-start.1
  7.3 0.9 constant_dynamic-slice_fusion.4
  8.2 0.1 pad_maximum_fusion.3
  8.3 82.5 %all_gather.16 = bf16[3072,96]{1,0:T(8,128)(2,1)S(1)} all-gather(bf16[16,96]{1,0:T(8,128)(2,1)S(1)} %pad_maximum_fusion.3), channel_id=1, replica_groups=mesh['fs_0'=12,'fs_1'=8,'fs_2'=2,'tp'=4] {'fs_0','fs_1','fs_2'}, dimensions={0}, use_global_device_ids=true | all-gather | bytes 592896 | tf_op jit(solution)/shard_map/all_gather | solution.py:22
  90.8 5.3 %convolution_convert_fusion = bf16[48,1024]{1,0:T(8,128)(2,1)S(1)} fusion(bf16[1024,3072]{1,0:T(8,128)(2,1)} %param.11, bf16[3072,96]{1,0:T(8,128)(2,1)S(1)} %all_gather.16), kind=kOutput, calls=%fused_computation | convolution fusion | flops 302039040 | bytes 6979584 | tf_op jit(solution)/shard_map/dot_general | solution.py:97
  96.1 0.0 copy-start.2
  96.1 0.0 copy-start.5
  96.1 0.0 copy-start.6
  96.1 0.0 copy-start.7
  96.2 0.0 copy-start.8
  96.2 2.0 convolution_convert_fusion.1
  98.2 0.0 copy-start.3
  98.2 0.0 copy-start.10
  98.2 0.0 copy-start.4
  98.2 0.0 copy-start.9
  98.3 12.0 %all_gather.17 = bf16[192,2048]{1,0:T(8,128)(2,1)S(1)} all-gather(bf16[48,2048]{1,0:T(8,128)(2,1)S(1)} %pad_maximum_fusion.1), channel_id=1, replica_groups=mesh['fs_0'=12,'fs_1'=8,'fs_2'=2,'tp'=4] {'tp'}, dimensions={0}, use_global_device_ids=true | all-gather | bytes 983040 | tf_op jit(solution)/shard_map/all_gather | solution.py:29
  110.3 0.4 fusion.2
  110.6 0.0 copy-done.2
  110.6 0.3 fusion.4
  111.0 0.9 pad_maximum_fusion
  111.9 0.0 reduce-scatter.2.cloned.1.call-update
  111.9 0.0 all-reduce.2.cloned.1.call-start
  112.0 16.6 %reduce-scatter.2.cloned.1.call-done = f32[96,576]{1,0:T(8,128)} async-done(((f32[192,576]{1,0:T(8,128)}), f32[96,576]{1,0:T(8,128)}) %reduce-scatter.2.cloned.1.call-update) | async-done | bytes 221200 | tf_op jit(solution)/shard_map/reduce_scatter | solution.py:49
  128.6 0.0 all-reduce.2.cloned.1.call-update
  128.6 0.0 all-gather.3.cloned.1.call-start
  128.7 0.1 concatenate.15
  128.8 76.3 %all-gather = f32[192,1,1152]{2,1,0:T(1,128)S(1)} all-gather(f32[1,1,1152]{2,1,0:T(1,128)S(1)} %bitcast.16), channel_id=1, replica_groups=mesh['fs_0'=12,'fs_1'=8,'fs_2'=2,'tp'=4] {'fs_0','fs_1','fs_2'}, dimensions={0}, use_global_device_ids=true | all-gather | bytes 889344 | tf_op jit(solution)/shard_map/all_gather | solution.py:22
  205.1 0.1 copy.29
  205.1 144.3 %all-reduce.2.cloned.1.call-done = f32[96,576]{1,0:T(8,128)} async-done(((f32[96,576]{1,0:T(8,128)}), f32[96,576]{1,0:T(8,128)}) %all-reduce.2.cloned.1.call-update) | async-done | bytes 221200 | tf_op jit(solution)/shard_map/psum | solution.py:50
  349.5 9.7 %all_gather.18 = f32[192,576]{1,0:T(8,128)S(1)} all-gather(f32[96,576]{1,0:T(8,128)} %all-reduce.2.cloned.1.call-done), channel_id=1, replica_groups=mesh['fs_0'=12,'fs_1'=8,'fs_2'=2,'tp'=4] {'fs_2'}, dimensions={0}, use_global_device_ids=true | all-gather | bytes 663552 | tf_op jit(solution)/shard_map/all_gather | solution.py:51
  359.2 0.8 multiply_reduce_fusion.1
  360.0 0.9 multiply_reduce_fusion
  362.2 7.9 %all_to_all.6 = f32[4,1,1]{2,1,0:T(1,128)S(1)} all-to-all(f32[4,1,1]{2,1,0:T(1,128)S(1)} %broadcast_in_dim.2), channel_id=1, replica_groups=mesh['fs_0'=12,'fs_1'=8,'fs_2'=2,'tp'=4] {'tp'}, dimensions={0} | all-to-all | bytes 32 | tf_op jit(solution)/shard_map/all_to_all | solution.py:57
  370.1 0.6 reduce_sum.29
  371.4 0.8 fusion.12
  372.2 0.9 fusion.13
  373.1 0.7 pad_maximum_fusion.2
  373.7 0.0 all-gather.3.cloned.1.call-update
  373.8 0.6 constant_dynamic-slice_fusion.3
  374.4 0.6 constant_dynamic-slice_fusion.2
  374.9 0.6 constant_dynamic-slice_fusion.1
  375.5 0.6 constant_dynamic-slice_fusion
  376.1 118.3 %all-gather.3.cloned.1.call-done = bf16[3072,576]{1,0:T(8,128)(2,1)} async-done(((bf16[16,576]{1,0:T(8,128)(2,1)}), bf16[3072,576]{1,0:T(8,128)(2,1)}) %all-gather.3.cloned.1.call-update) | async-done | bytes 3538960 | tf_op jit(solution)/shard_map/all_gather | solution.py:22
  494.3 1.5 split.48
  495.9 1.5 copy.25
  497.3 4.6 split.49
  (12 shorter events, 0.0 us)
Async XLA Ops:
  7.2 103.1 %copy-start = (bf16[1024,384]{1,0:T(8,128)(2,1)S(1)}, bf16[1024,384]{1,0:T(8,128)(2,1)}, u32[]{:S(2)}) copy-start(bf16[1024,384]{1,0:T(8,128)(2,1)} %param.13) | copy-start | bytes 2359300
  7.2 121.4 %reduce-scatter.2.cloned.1.call-start = ((), (), s32[]{:S(2)}) async-start(), calls=%async_computation.2 | async-start | bytes 737280 | tf_op jit(solution)/shard_map/reduce_scatter | solution.py:49
  7.2 88.9 %copy-start.1 = (bf16[1024,3072]{1,0:T(8,128)(2,1)S(1)}, bf16[1024,3072]{1,0:T(8,128)(2,1)}, u32[]{:S(2)}) copy-start(bf16[1024,3072]{1,0:T(8,128)(2,1)} %param.11) | copy-start | bytes 18874372
  96.1 14.5 %copy-start.2 = (bf16[1024,192]{0,1:T(8,128)(2,1)S(1)}, bf16[1024,192]{0,1:T(8,128)(2,1)}, u32[]{:S(2)}) copy-start(bf16[1024,192]{0,1:T(8,128)(2,1)} %param.12) | copy-start | bytes 1179652
  96.1 32.5 %copy-start.5 = (f32[1,384]{1,0:T(1,128)S(1)}, f32[1,384]{1,0:T(1,128)}, u32[]{:S(2)}) copy-start(f32[1,384]{1,0:T(1,128)} %param.20) | copy-start | bytes 4612
  96.1 32.5 %copy-start.6 = (f32[1,384]{1,0:T(1,128)S(1)}, f32[1,384]{1,0:T(1,128)}, u32[]{:S(2)}) copy-start(f32[1,384]{1,0:T(1,128)} %param.21) | copy-start | bytes 4612
  96.1 32.5 %copy-start.7 = (f32[1,192]{1,0:T(1,128)S(1)}, f32[1,192]{1,0:T(1,128)}, u32[]{:S(2)}) copy-start(f32[1,192]{1,0:T(1,128)} %param.18) | copy-start | bytes 2308
  96.2 32.5 %copy-start.8 = (f32[1,192]{1,0:T(1,128)S(1)}, f32[1,192]{1,0:T(1,128)}, u32[]{:S(2)}) copy-start(f32[1,192]{1,0:T(1,128)} %param.19) | copy-start | bytes 2308
  98.2 273.2 %copy-start.3 = (bf16[16,192]{1,0:T(8,128)(2,1)S(1)}, bf16[16,192]{1,0:T(8,128)(2,1)}, u32[]{:S(2)}) copy-start(bf16[16,192]{1,0:T(8,128)(2,1)} %param.14) | copy-start | bytes 18436
  98.2 273.2 %copy-start.10 = (f32[16,192]{1,0:T(8,128)S(1)}, f32[16,192]{1,0:T(8,128)}, u32[]{:S(2)}) copy-start(f32[16,192]{1,0:T(8,128)} %param.16) | copy-start | bytes 36868
  98.2 274.0 %copy-start.4 = (bf16[16,192]{1,0:T(8,128)(2,1)S(1)}, bf16[16,192]{1,0:T(8,128)(2,1)}, u32[]{:S(2)}) copy-start(bf16[16,192]{1,0:T(8,128)(2,1)} %param.15) | copy-start | bytes 18436
  98.2 274.0 %copy-start.9 = (f32[16,384]{1,0:T(8,128)S(1)}, f32[16,384]{1,0:T(8,128)}, u32[]{:S(2)}) copy-start(f32[16,384]{1,0:T(8,128)} %param.17) | copy-start | bytes 73732
  111.9 237.6 %all-reduce.2.cloned.1.call-start = ((), (), s32[]{:S(2)}) async-start(), calls=%async_computation.3 | async-start | bytes 491520 | tf_op jit(solution)/shard_map/psum | solution.py:50
  128.6 365.7 %all-gather.3.cloned.1.call-start = ((), (), s32[]{:S(2)}) async-start(), calls=%async_computation.4 | async-start | bytes 3952640 | tf_op jit(solution)/shard_map/all_gather | solution.py:22
Sparse Core Ops, SparseCore 0:
  112.0 16.4 reduce-scatter.1
  132.2 217.2 all-reduce.1
  373.9 120.4 all-gather.2
where the time goes:
time: 509 us; the launch traced here: 508 us
  waiting for transfers between devices  279 us (55%)
  blocking collectives  188 us (37%)
  between operations  16 us (3%)
  local copies, waits for them, and re-layouts  11 us (2%)
  matrix products  9.65 us (2%)
    all_gather x2, blocking collectives, in_one_piece(): lax.all_gather(both, axis, axis=dim, tiled=True)  159 us
    psum x1, waiting for transfers between devices, sum_by_parts(): own = lax.psum(own, far)  144 us
    all_gather x1, waiting for transfers between devices, in_one_piece(): lax.all_gather(both, axis, axis=dim, tiled=True)  118 us
    reduce_scatter x1, waiting for transfers between devices, sum_by_parts(): own = lax.psum_scatter(padded, near, scatter_dimension=0, tiled=True)  16.6 us
    all_gather x1, blocking collectives, rows_first(): whole = lax.all_gather(both, axis, axis=0, tiled=True)  12 us
  transfers between devices with their start and end apart: 3, of which 3 were waited for; matrix products, arithmetic and copies ran while one was open for 0% of the time, Pallas kernels for 0%

commit v1 on v0

v1 whole, which is shorter than its diff:
```python
import jax
import jax.numpy as jnp
from jax import lax
from jax.sharding import Mesh
from jax.sharding import PartitionSpec as P

FS = ("fs_0", "fs_1", "fs_2")


first_decay = 0.9
second_decay = 0.99
small_eps = 1e-08
learn_rate = 0.01


def sent_to_all(value, axis):
    size = lax.axis_size(axis)
    return lax.all_to_all(
        jnp.broadcast_to(value[None], (size, *value.shape)), axis, 0, 0, tiled=True
    )


def summed_share(value, axis):
    size = lax.axis_size(axis)
    parts = value.reshape(size, -1, *value.shape[1:])
    return lax.all_to_all(parts, axis, 0, 0, tiled=True).sum(axis=0)


def moments(old_first, old_second, gradient):
    first = first_decay * old_first + (1.0 - first_decay) * gradient
    second = second_decay * old_second + (1.0 - second_decay) * gradient * gradient
    unit = first / (jnp.sqrt(second) + small_eps)
    return (first, second, unit)


def pieces_of(value):
    pieces = []
    for _ in range(3):
        piece = lax.reduce_precision(value, 8, 7)
        pieces.append(piece.astype(jnp.bfloat16))
        value = value - piece
    return pieces


def turned_cols(rank, begin, width):
    n0, n1, n2 = (lax.axis_size(a) for a in FS)
    place = begin + lax.broadcasted_iota(jnp.int32, (rank, width), 1)
    core, rest = place // (n0 * n1), place % (n0 * n1)
    natural = (rest // n1) * (n1 * n2) + (rest % n1) * n2 + core
    row = lax.broadcasted_iota(jnp.int32, (rank, width), 0)
    return (row == natural).astype(jnp.bfloat16)


def exact(a, onehot):
    return jnp.dot(a, onehot, preferred_element_type=jnp.float32).astype(jnp.bfloat16)


def on_device(
    inputs,
    query_cot,
    value_cot,
    query_factor,
    value_factor,
    query_weight,
    value_weight,
    query_first,
    query_second,
    value_first,
    value_second,
):
    n0, n1, n2 = (lax.axis_size(a) for a in FS)
    tp = lax.axis_size("tp")
    own, rank = query_factor.shape
    q_cols = query_cot.shape[1]
    v_cols = value_cot.shape[1]
    cols = q_cols + v_cols
    entries = rank * cols * tp
    width = rank // tp
    bf16 = jnp.bfloat16

    turn = turned_cols(rank, 0, rank)
    factors = exact(jnp.concatenate([value_factor, query_factor], axis=0), turn)
    v_factor, q_factor = factors[:own], factors[own:]

    parcel = jnp.concatenate(
        [v_factor, q_factor, value_weight.astype(bf16), query_weight.astype(bf16)], axis=1
    )
    parcels = lax.all_gather(parcel, FS, axis=0, tiled=True)

    mine = turned_cols(rank, lax.axis_index("tp") * width, width)
    share = exact(jnp.concatenate([value_factor, query_factor], axis=0), mine)
    share = jnp.concatenate([share[:own], share[own:]], axis=1)
    near = sent_to_all(share, "fs_0")
    near = sent_to_all(near, "fs_1")
    near = sent_to_all(near, "fs_2")
    share = near.transpose(2, 1, 0, 3, 4).reshape(-1, 2 * width)
    proj = lax.dot_general(
        share, inputs, (((0,), (1,)), ((), ())), preferred_element_type=jnp.float32
    ).astype(bf16)
    proj = lax.all_gather(proj, "tp", axis=0, tiled=True).reshape(tp, 2, width, -1)
    proj_v = proj[:, 0].reshape(rank, -1)
    proj_q = proj[:, 1].reshape(rank, -1)

    term_v = jnp.dot(proj_v, value_cot, preferred_element_type=jnp.float32)
    term_q = jnp.dot(proj_q, query_cot, preferred_element_type=jnp.float32)
    term = jnp.concatenate([term_v, term_q], axis=1)
    term = summed_share(term, "fs_2")
    term = summed_share(term, "fs_0")
    term = summed_share(term, "fs_1")
    first_v, second_v, unit_v = moments(value_first, value_second, term[:, :v_cols])
    first_q, second_q, unit_q = moments(query_first, query_second, term[:, v_cols:])

    squares = jnp.sum(unit_v * unit_v, axis=1, keepdims=True)
    squares += jnp.sum(unit_q * unit_q, axis=1, keepdims=True)
    spare = -(cols + 3) % 128
    row = jnp.concatenate(
        [
            unit_v.astype(bf16),
            unit_q.astype(bf16),
            *pieces_of(squares),
            jnp.zeros((1, spare), bf16),
        ],
        axis=1,
    )
    rows = sent_to_all(row[0], ("fs_1", "tp")).reshape(n1, tp, -1)
    squares = jnp.sum(rows[:, :, cols : cols + 3].astype(jnp.float32), axis=(1, 2))[:, None]
    rows = lax.dynamic_index_in_dim(rows, lax.axis_index("tp"), 1, keepdims=False)
    rows = jnp.concatenate([rows[:, :cols], *pieces_of(squares), rows[:, cols + 3 :]], axis=1)
    rows = sent_to_all(rows, "fs_0").reshape(n0 * n1, -1)
    rows = sent_to_all(rows, "fs_2").reshape(rank, -1)
    total = jnp.sum(rows[:, cols : cols + 3].astype(jnp.float32))
    scale = lax.rsqrt(total / entries + 1e-06)
    rows_v = rows[:, :v_cols]
    rows_q = rows[:, v_cols:cols]

    step_v = scale * jnp.dot(v_factor, rows_v, preferred_element_type=jnp.float32)
    step_q = scale * jnp.dot(q_factor, rows_q, preferred_element_type=jnp.float32)
    new_v = value_weight - learn_rate * step_v
    new_q = query_weight - learn_rate * step_q

    both = parcels[:, : 2 * rank]
    weights = parcels[:, 2 * rank :].astype(jnp.float32)
    pad_v = jnp.concatenate([rows_v, jnp.zeros_like(rows_v)], axis=0)
    pad_q = jnp.concatenate([jnp.zeros_like(rows_q), rows_q], axis=0)
    rate = learn_rate * scale
    all_v = jnp.dot(both, pad_v, preferred_element_type=jnp.float32)
    all_q = jnp.dot(both, pad_q, preferred_element_type=jnp.float32)
    copy_v = (weights[:, :v_cols] - rate * all_v).astype(bf16)
    copy_q = (weights[:, v_cols:] - rate * all_q).astype(bf16)
    return (step_q, step_v, new_q, new_v, first_q, second_q, first_v, second_v, copy_q, copy_v)


def solution(mesh):
    split = Mesh(mesh.devices.reshape(12, 8, 2, mesh.shape["tp"]), ("fs_0", "fs_1", "fs_2", "tp"))
    return jax.shard_map(
        on_device,
        mesh=split,
        in_specs=(
            P(FS, None),
            P(FS, "tp"),
            P(FS, "tp"),
            P(FS, None),
            P(FS, None),
            P(FS, "tp"),
            P(FS, "tp"),
            P(FS, "tp"),
            P(FS, "tp"),
            P(FS, "tp"),
            P(FS, "tp"),
        ),
        out_specs=(
            P(FS, "tp"),
            P(FS, "tp"),
            P(FS, "tp"),
            P(FS, "tp"),
            P(FS, "tp"),
            P(FS, "tp"),
            P(FS, "tp"),
            P(FS, "tp"),
            P(None, "tp"),
            P(None, "tp"),
        ),
        check_vma=False,
    )
```

time: 509 us -> 312 us (0.61)
  waiting for transfers between devices: 279 us -> 152 us
  blocking collectives: 188 us -> 79.4 us
  starting transfers between devices: 0.12 us -> 16 us
  local copies, waits for them, and re-layouts: 11 us -> 22.1 us
    all_gather x4 -> x1, blocking collectives: 181 us -> 12.1 us  [on_device(): lax.all_gather(proj, 'tp', axis=0, tiled=True).reshape(tp, 2, width, -1)]
    psum x1 -> x0, waiting for transfers between devices: 144 us -> none  [sum_by_parts(): own = lax.psum(own, far)]
    all_to_all x1 -> x4, blocking collectives: 7.9 us -> 61.3 us  [sent_to_all(): lax.all_to_all(jnp.broadcast_to(value[None], (size, *value.shape)), axis,...]
    all_to_all x0 -> x4, waiting for transfers between devices: none -> 39.7 us  [the longest x2 20.7 us: summed_share(): return lax.all_to_all(parts, axis, 0, 0, tiled=True).sum(axis=0)]
    reduce_scatter x1 -> x0, waiting for transfers between devices: 16.6 us -> none  [sum_by_parts(): own = lax.psum_scatter(padded, near, scatter_dimension=0, tiled=True)]
    all_to_all x0 -> x4, starting transfers between devices: none -> 15.9 us  [the longest x2 9.04 us: sent_to_all(): lax.all_to_all(jnp.broadcast_to(value[None], (size, *value.shape)), axis,...]
    unnamed x24 -> x27, local copies, waits for them, and re-layouts: 1.6 us -> 13.2 us
    split x2 -> x0, local copies, waits for them, and re-layouts: 6.06 us -> none  [in_one_piece(): jnp.split(lax.all_gather(both, axis, axis=dim, tiled=True), ends, axis=al...]
  transfers between devices with their start and end apart: 3 -> 5, of which waited for: 3 -> 5; matrix products, arithmetic and copies ran while one was open for 0% -> 0% of each run, Pallas kernels for 0% -> 0%
where the time goes in v1:
time: 312 us; the launch traced here: 311 us
  waiting for transfers between devices  152 us (49%)
  blocking collectives  79.4 us (25%)
  local copies, waits for them, and re-layouts  22.1 us (7%)
  between operations  20.5 us (7%)
  starting transfers between devices  16 us (5%)
  matrix products  12.2 us (4%)
  other arithmetic  8.87 us (3%)
    all_gather x1, waiting for transfers between devices, on_device(): parcels = lax.all_gather(parcel, FS, axis=0, tiled=True)  112 us
    all_to_all x4, blocking collectives, sent_to_all(): lax.all_to_all(jnp.broadcast_to(value[None], (size, *value.shape)), axis,...  61.3 us
    all_to_all x2, waiting for transfers between devices, summed_share(): return lax.all_to_all(parts, axis, 0, 0, tiled=True).sum(axis=0)  20.7 us
    all_to_all x2, waiting for transfers between devices, sent_to_all(): lax.all_to_all(jnp.broadcast_to(value[None], (size, *value.shape)), axis,...  18.9 us
    unnamed x27, local copies, waits for them, and re-layouts  13.2 us
    all_gather x1, blocking collectives, on_device(): lax.all_gather(proj, 'tp', axis=0, tiled=True).reshape(tp, 2, width, -1)  12.1 us
    all_to_all x2, starting transfers between devices, sent_to_all(): lax.all_to_all(jnp.broadcast_to(value[None], (size, *value.shape)), axis,...  9.04 us
    all_to_all x2, starting transfers between devices, summed_share(): return lax.all_to_all(parts, axis, 0, 0, tiled=True).sum(axis=0)  6.88 us
  transfers between devices with their start and end apart: 5, of which 5 were waited for; matrix products, arithmetic and copies ran while one was open for 0% of the time, Pallas kernels for 0%

profile of v1, /device:TPU:1, one launch (start us, length us, event | category | flops | bytes accessed | tf_op | source)
XLA Modules:
  0.0 310.9 jit_solution(11379244283684242332)
XLA Ops:
  7.3 0.9 constant_dynamic-update-slice_fusion.1
  8.1 0.9 constant_dynamic-update-slice_fusion
  9.1 0.2 convolution_convert_fusion.2
  9.3 25.2 %all_to_all.46 = bf16[12,16,96]{2,1,0:T(8,128)(2,1)S(1)} all-to-all(bf16[12,16,96]{2,1,0:T(8,128)(2,1)S(1)} %broadcast_in_dim.16), channel_id=1, replica_groups=mesh['fs_0'=12,'fs_1'=8,'fs_2'=2,'tp'=4] {'fs_0'}, dimensions={0} | all-to-all | bytes 73728 | tf_op jit(solution)/shard_map/all_to_all | solution.py:18
  34.6 18.2 %all_to_all.47 = bf16[8,12,16,96]{3,2,1,0:T(8,128)(2,1)S(1)} all-to-all(bf16[8,12,16,96]{3,2,1,0:T(8,128)(2,1)S(1)} %broadcast_in_dim.17), channel_id=1, replica_groups=mesh['fs_0'=12,'fs_1'=8,'fs_2'=2,'tp'=4] {'fs_1'}, dimensions={0} | all-to-all | bytes 589824 | tf_op jit(solution)/shard_map/all_to_all | solution.py:18
  52.8 0.2 broadcast_in_dim.18
  53.0 8.0 %all_to_all.48 = bf16[2,8,12,16,96]{4,3,1,2,0:T(8,128)(2,1)S(1)} all-to-all(bf16[2,8,12,16,96]{4,3,1,2,0:T(8,128)(2,1)S(1)} %broadcast_in_dim.18), channel_id=1, replica_groups=mesh['fs_0'=12,'fs_1'=8,'fs_2'=2,'tp'=4] {'fs_2'}, dimensions={0} | all-to-all | bytes 1179648 | tf_op jit(solution)/shard_map/all_to_all | solution.py:18
  61.0 0.1 copy.64
  61.2 2.1 convolution_convert_fusion
  63.3 12.1 %all_gather.6 = bf16[384,1024]{1,0:T(8,128)(2,1)S(1)} all-gather(bf16[96,1024]{1,0:T(8,128)(2,1)S(1)} %convolution_convert_fusion), channel_id=1, replica_groups=mesh['fs_0'=12,'fs_1'=8,'fs_2'=2,'tp'=4] {'tp'}, dimensions={0}, use_global_device_ids=true | all-gather | bytes 983040 | tf_op jit(solution)/shard_map/all_gather | solution.py:100
  75.6 0.4 fusion.92
  75.9 0.3 fusion.93
  76.3 6.0 %all_to_all.49 = f32[2,96,576]{2,1,0:T(8,128)S(1)} all-to-all(f32[2,96,576]{2,1,0:T(8,128)S(1)} %bitcast.32), channel_id=1, replica_groups=mesh['fs_0'=12,'fs_1'=8,'fs_2'=2,'tp'=4] {'fs_2'}, dimensions={0} | all-to-all | bytes 884736 | tf_op jit(solution)/shard_map/all_to_all | solution.py:26
  82.3 0.7 reduce_sum.67
  83.0 3.5 %all-to-all-start.4 = ((f32[12,8,576]{2,1,0:T(8,128)}), f32[12,8,576]{2,1,0:T(8,128)S(1)}, u32[]{:S(2)}, u32[]{:S(2)}) async-start(f32[12,8,576]{2,1,0:T(8,128)} %bitcast.6), calls=%async_computation.4 | async-start | bytes 491520 | tf_op jit(solution)/shard_map/all_to_all | solution.py:26
  86.6 14.2 %all-to-all-done.4 = f32[12,8,576]{2,1,0:T(8,128)S(1)} async-done(((f32[12,8,576]{2,1,0:T(8,128)}), f32[12,8,576]{2,1,0:T(8,128)S(1)}, u32[]{:S(2)}, u32[]{:S(2)}) %all-to-all-start.4) | async-done | bytes 221216 | tf_op jit(solution)/shard_map/all_to_all | solution.py:26
  100.7 0.6 copy.65
  101.4 3.3 %all-to-all-start.5 = ((f32[8,1,576]{2,1,0:T(1,128)}), f32[8,1,576]{2,1,0:T(1,128)S(1)}, u32[]{:S(2)}, u32[]{:S(2)}) async-start(f32[8,1,576]{2,1,0:T(1,128)} %copy.65), calls=%async_computation.5 | async-start | bytes 40960 | tf_op jit(solution)/shard_map/all_to_all | solution.py:26
  104.7 6.6 %all-to-all-done.5 = f32[8,1,576]{2,1,0:T(1,128)S(1)} async-done(((f32[8,1,576]{2,1,0:T(1,128)}), f32[8,1,576]{2,1,0:T(1,128)S(1)}, u32[]{:S(2)}, u32[]{:S(2)}) %all-to-all-start.5) | async-done | bytes 18464 | tf_op jit(solution)/shard_map/all_to_all | solution.py:26
  111.3 1.2 multiply_reduce_fusion.1
  112.5 1.2 multiply_reduce_fusion
  119.1 0.7 concatenate.30
  119.9 0.5 broadcast.96
  120.5 0.9 reduce.5
  121.3 0.7 reshape.112
  122.1 4.6 %all-to-all-start.6 = ((bf16[32,2,320]{2,1,0:T(2,128)(2,1)}), bf16[32,2,320]{2,1,0:T(2,128)(2,1)S(1)}, u32[]{:S(2)}, u32[]{:S(2)}) async-start(bf16[32,2,320]{2,1,0:T(2,128)(2,1)} %reshape.112), calls=%async_computation.6 | async-start | bytes 98304 | tf_op jit(solution)/shard_map/all_to_all | solution.py:18
  126.6 8.7 %all-to-all-done.6 = bf16[32,2,320]{2,1,0:T(2,128)(2,1)S(1)} async-done(((bf16[32,2,320]{2,1,0:T(2,128)(2,1)}), bf16[32,2,320]{2,1,0:T(2,128)(2,1)S(1)}, u32[]{:S(2)}, u32[]{:S(2)}) %all-to-all-start.6) | async-done | bytes 40992 | tf_op jit(solution)/shard_map/all_to_all | solution.py:18
  135.4 0.1 reshape.113
  135.5 0.2 reduce.4
  135.7 0.2 convert_reduce_fusion
  136.2 0.1 concatenate.32
  136.2 0.7 broadcast_in_dim.21
  136.9 4.5 %all-to-all-start.7 = ((bf16[12,8,640]{2,1,0:T(8,128)(2,1)}), bf16[12,8,640]{2,1,0:T(8,128)(2,1)S(1)}, u32[]{:S(2)}, u32[]{:S(2)}) async-start(bf16[12,8,640]{2,1,0:T(8,128)(2,1)} %broadcast_in_dim.21), calls=%async_computation.7 | async-start | bytes 245760 | tf_op jit(solution)/shard_map/all_to_all | solution.py:18
  141.4 0.2 convolution_convert_fusion.1
  141.6 10.2 %all-to-all-done.7 = bf16[12,8,640]{2,1,0:T(8,128)(2,1)S(1)} async-done(((bf16[12,8,640]{2,1,0:T(8,128)(2,1)}), bf16[12,8,640]{2,1,0:T(8,128)(2,1)S(1)}, u32[]{:S(2)}, u32[]{:S(2)}) %all-to-all-start.7) | async-done | bytes 122912 | tf_op jit(solution)/shard_map/all_to_all | solution.py:18
  151.9 9.9 %all_to_all.50 = bf16[2,96,640]{2,1,0:T(8,128)(2,1)S(1)} all-to-all(bf16[2,96,640]{2,1,0:T(8,128)(2,1)S(1)} %broadcast_in_dim.23), channel_id=1, replica_groups=mesh['fs_0'=12,'fs_1'=8,'fs_2'=2,'tp'=4] {'fs_2'}, dimensions={0} | all-to-all | bytes 491520 | tf_op jit(solution)/shard_map/all_to_all | solution.py:18
  161.9 0.6 convert_reduce_fusion.1
  163.2 0.8 fusion.90
  164.0 0.8 fusion.88
  164.8 0.7 pad_maximum_fusion.1
  165.5 112.3 %all-gather.2.cloned.1.call-done = bf16[3072,960]{1,0:T(8,128)(2,1)} async-done(((bf16[16,960]{1,0:T(8,128)(2,1)}), bf16[3072,960]{1,0:T(8,128)(2,1)}) %all-gather.2.cloned.1.call-update) | async-done | bytes 5898256 | tf_op jit(solution)/shard_map/all_gather | solution.py:88
  277.8 4.4 %slice.86 = bf16[3072,576]{1,0:T(8,128)(2,1)} slice(bf16[3072,960]{1,0:T(8,128)(2,1)} %all-gather.2.cloned.1.call-done), slice={[0:3072], [384:960]} | slice | bytes 7077888 | tf_op jit(solution)/shard_map/slice | solution.py:142
  282.2 6.0 %copy.76 = bf16[3072,576]{0,1:T(8,128)(2,1)} copy(bf16[3072,576]{1,0:T(8,128)(2,1)} %slice.86) | data formatting | bytes 7077888
  288.2 2.9 convert_element_type.95
  291.1 2.9 copy-done.1
  294.1 3.2 %fusion = bf16[3072,384]{0,1:T(8,128)(2,1)S(1)} fusion(f32[3072,576]{0,1:T(8,128)S(1)} %convert_element_type.95, f32[]{:T(128)S(6)} %mul.163, bf16[3072,960]{1,0:T(8,128)(2,1)} %all-gather.2.cloned.1.call-done, bf16[192,384]{1,0:T(8,128)(2,1)S(1)} %slice.85), kind=kOutput, calls=%fused_computation.1 | convolution fusion | flops 909508608 | bytes 9584644 | tf_op jit(solution)/shard_map/dot_general | solution.py:146
  297.3 2.4 copy.71
  299.7 4.4 %fusion.2 = bf16[3072,192]{0,1:T(8,128)(2,1)} fusion(f32[3072,576]{0,1:T(8,128)} %copy-done.1, bf16[3072,960]{1,0:T(8,128)(2,1)} %all-gather.2.cloned.1.call-done, f32[]{:T(128)S(6)} %mul.163, bf16[192,192]{1,0:T(8,128)(2,1)S(1)} %slice.83), kind=kOutput, calls=%fused_computation.4 | convolution fusion | flops 454754304 | bytes 5971972 | tf_op jit(solution)/shard_map/dot_general | solution.py:147
  (52 shorter events, 1.0 us)
Async XLA Ops:
  7.2 68.3 %copy-start = (bf16[1024,384]{1,0:T(8,128)(2,1)S(1)}, bf16[1024,384]{1,0:T(8,128)(2,1)}, u32[]{:S(2)}) copy-start(bf16[1024,384]{1,0:T(8,128)(2,1)} %param.13) | copy-start | bytes 2359300
  7.2 54.0 %copy-start.2 = (bf16[1024,3072]{1,0:T(8,128)(2,1)S(1)}, bf16[1024,3072]{1,0:T(8,128)(2,1)}, u32[]{:S(2)}) copy-start(bf16[1024,3072]{1,0:T(8,128)(2,1)} %param.11) | copy-start | bytes 18874372
  61.2 14.7 %copy-start.3 = (bf16[1024,192]{0,1:T(8,128)(2,1)S(1)}, bf16[1024,192]{0,1:T(8,128)(2,1)}, u32[]{:S(2)}) copy-start(bf16[1024,192]{0,1:T(8,128)(2,1)} %param.12) | copy-start | bytes 1179652
  63.3 48.0 %copy-start.8 = (f32[1,192]{1,0:T(1,128)S(1)}, f32[1,192]{1,0:T(1,128)}, u32[]{:S(2)}) copy-start(f32[1,192]{1,0:T(1,128)} %param.19) | copy-start | bytes 2308
  63.3 48.0 %copy-start.9 = (f32[1,192]{1,0:T(1,128)S(1)}, f32[1,192]{1,0:T(1,128)}, u32[]{:S(2)}) copy-start(f32[1,192]{1,0:T(1,128)} %param.18) | copy-start | bytes 2308
  63.3 49.2 %copy-start.6 = (f32[1,384]{1,0:T(1,128)S(1)}, f32[1,384]{1,0:T(1,128)}, u32[]{:S(2)}) copy-start(f32[1,384]{1,0:T(1,128)} %param.21) | copy-start | bytes 4612
  63.3 49.2 %copy-start.7 = (f32[1,384]{1,0:T(1,128)S(1)}, f32[1,384]{1,0:T(1,128)}, u32[]{:S(2)}) copy-start(f32[1,384]{1,0:T(1,128)} %param.20) | copy-start | bytes 4612
  75.5 87.7 %copy-start.5 = (f32[16,192]{1,0:T(8,128)S(1)}, f32[16,192]{1,0:T(8,128)}, u32[]{:S(2)}) copy-start(f32[16,192]{1,0:T(8,128)} %param.16) | copy-start | bytes 36868
  75.5 88.5 %copy-start.4 = (f32[16,384]{1,0:T(8,128)S(1)}, f32[16,384]{1,0:T(8,128)}, u32[]{:S(2)}) copy-start(f32[16,384]{1,0:T(8,128)} %param.17) | copy-start | bytes 73732
  83.0 17.7 %all-to-all-start.4 = ((f32[12,8,576]{2,1,0:T(8,128)}), f32[12,8,576]{2,1,0:T(8,128)S(1)}, u32[]{:S(2)}, u32[]{:S(2)}) async-start(f32[12,8,576]{2,1,0:T(8,128)} %bitcast.6), calls=%async_computation.4 | async-start | bytes 491520 | tf_op jit(solution)/shard_map/all_to_all | solution.py:26
  101.4 9.9 %all-to-all-start.5 = ((f32[8,1,576]{2,1,0:T(1,128)}), f32[8,1,576]{2,1,0:T(1,128)S(1)}, u32[]{:S(2)}, u32[]{:S(2)}) async-start(f32[8,1,576]{2,1,0:T(1,128)} %copy.65), calls=%async_computation.5 | async-start | bytes 40960 | tf_op jit(solution)/shard_map/all_to_all | solution.py:26
  122.1 13.3 %all-to-all-start.6 = ((bf16[32,2,320]{2,1,0:T(2,128)(2,1)}), bf16[32,2,320]{2,1,0:T(2,128)(2,1)S(1)}, u32[]{:S(2)}, u32[]{:S(2)}) async-start(bf16[32,2,320]{2,1,0:T(2,128)(2,1)} %reshape.112), calls=%async_computation.6 | async-start | bytes 98304 | tf_op jit(solution)/shard_map/all_to_all | solution.py:18
  136.9 14.9 %all-to-all-start.7 = ((bf16[12,8,640]{2,1,0:T(8,128)(2,1)}), bf16[12,8,640]{2,1,0:T(8,128)(2,1)S(1)}, u32[]{:S(2)}, u32[]{:S(2)}) async-start(bf16[12,8,640]{2,1,0:T(8,128)(2,1)} %broadcast_in_dim.21), calls=%async_computation.7 | async-start | bytes 245760 | tf_op jit(solution)/shard_map/all_to_all | solution.py:18
  141.4 136.4 %all-gather.2.cloned.1.call-start = ((), (), s32[]{:S(2)}) async-start(), calls=%async_computation.9 | async-start | bytes 6324224 | tf_op jit(solution)/shard_map/all_gather | solution.py:88
  291.1 2.9 copy-start.1
Sparse Core Ops, SparseCore 0:
  165.6 112.1 all-gather.1

commit v2 on v1

v2 whole, which is shorter than its diff:
```python
import math

import jax
import jax.numpy as jnp
from jax import lax
from jax.experimental import pallas as pl
from jax.experimental.pallas import tpu as pltpu
from jax.sharding import Mesh
from jax.sharding import PartitionSpec as P

FS = ("fs_0", "fs_1", "fs_2")


first_decay = 0.9
second_decay = 0.99
small_eps = 1e-08
learn_rate = 0.01


def sent_to_all(value, axis):
    size = lax.axis_size(axis)
    return lax.all_to_all(
        jnp.broadcast_to(value[None], (size, *value.shape)), axis, 0, 0, tiled=True
    )


def summed_share(value, axis):
    size = lax.axis_size(axis)
    parts = value.reshape(size, -1, *value.shape[1:])
    return lax.all_to_all(parts, axis, 0, 0, tiled=True).sum(axis=0)


def shift_of(size):
    shift = int(math.log2(size))
    assert 1 << shift == size
    return shift


def pack_kernel(at, v_factor, q_factor, v_weight, q_weight, parcel, spread, *, sizes, width):
    own, rank = v_factor.shape
    n0, n1, n2 = sizes
    row = lax.broadcasted_iota(jnp.int32, (rank, rank), 0)
    place = (
        (row & (n2 - 1)) * (n0 * n1)
        + (row >> shift_of(n1 * n2)) * n1
        + ((row >> shift_of(n2)) & (n1 - 1))
    )
    col = lax.broadcasted_iota(jnp.int32, (rank, rank), 1)
    turn = (place == col).astype(jnp.float32).astype(jnp.bfloat16)
    mine = (place == col + at[0] * width) & (col < width)
    mine = mine.astype(jnp.float32).astype(jnp.bfloat16)

    def exact(a, onehot):
        return jnp.dot(a, onehot, preferred_element_type=jnp.float32).astype(jnp.bfloat16)

    vf, qf = v_factor[...], q_factor[...]
    parcel[...] = jnp.concatenate(
        [
            exact(vf, turn),
            exact(qf, turn),
            v_weight[...].astype(jnp.bfloat16),
            q_weight[...].astype(jnp.bfloat16),
        ],
        axis=1,
    )
    share = jnp.concatenate([exact(vf, mine)[:, :width], exact(qf, mine)[:, :width]], axis=1)
    spread[...] = jnp.broadcast_to(share[None], spread.shape)


def pieces_of(value):
    high = value.astype(jnp.bfloat16).astype(jnp.float32)
    middle = (value - high).astype(jnp.bfloat16).astype(jnp.float32)
    return high, middle, value - high - middle


def with_pieces(value, block, at):
    lane = lax.broadcasted_iota(jnp.int32, block.shape, 1)
    for k, piece in enumerate(pieces_of(value)):
        block = jnp.where(lane == at + k, piece, block)
    return block


def moments(old_first, old_second, gradient):
    first = first_decay * old_first + (1.0 - first_decay) * gradient
    second = second_decay * old_second + (1.0 - second_decay) * gradient * gradient
    unit = first / (jnp.sqrt(second) + small_eps)
    return (first, second, unit)


def moments_kernel(terms, v_first, v_second, q_first, q_second, *outs):
    first_v, second_v, first_q, second_q, spread = outs
    v_cols = v_first.shape[1]
    gradient = jnp.sum(terms[...], axis=0)
    first_v[...], second_v[...], unit_v = moments(v_first[...], v_second[...], gradient[:, :v_cols])
    first_q[...], second_q[...], unit_q = moments(q_first[...], q_second[...], gradient[:, v_cols:])
    squares = jnp.sum(unit_v * unit_v, axis=1, keepdims=True)
    squares += jnp.sum(unit_q * unit_q, axis=1, keepdims=True)
    cols = gradient.shape[1]
    lines = -(-(cols + 3) // 128)
    row = jnp.concatenate(
        [unit_v, unit_q, jnp.zeros((1, lines * 128 - cols), jnp.float32)], axis=1
    )
    row = with_pieces(squares, row, cols)
    block = jnp.concatenate(
        [row[:, 128 * k : 128 * (k + 1)] for k in range(lines)]
        + [jnp.zeros((spread.shape[1] - lines, 128), jnp.float32)],
        axis=0,
    ).astype(jnp.bfloat16)
    spread[...] = jnp.broadcast_to(block[None], spread.shape)


def regroup_kernel(at, blocks, spread, *, cols):
    n1, tp = blocks.shape[:2]
    lines = spread.shape[2] // 128
    last, begin = cols // 128, cols % 128
    ends = blocks[:, :, last, :].astype(jnp.float32)
    ends = jnp.sum(ends, axis=1)
    lane = lax.broadcasted_iota(jnp.int32, ends.shape, 1)
    squares = jnp.where((lane >= begin) & (lane < begin + 3), ends, 0.0)
    squares = jnp.sum(squares, axis=1, keepdims=True)
    own = blocks[:, at[0], :, :].astype(jnp.float32)
    parts = [own[:, k, :] for k in range(lines)]
    parts[last] = with_pieces(squares, parts[last], begin)
    rows = jnp.concatenate(parts, axis=1).astype(jnp.bfloat16)
    spread[...] = jnp.broadcast_to(rows[None], spread.shape)


def update_kernel(
    rows, own, v_weight, q_weight, parcels, step_v, step_q, new_v, new_q, copy_v, copy_q, units,
    *, rank, v_cols, q_cols, entries
):
    cols = v_cols + q_cols
    tail = rows[:, cols // 128 * 128 :].astype(jnp.float32)
    lane = lax.broadcasted_iota(jnp.int32, tail.shape, 1) + cols // 128 * 128
    total = jnp.sum(jnp.where((lane >= cols) & (lane < cols + 3), tail, 0.0), keepdims=True)
    scale = lax.rsqrt(total / entries + 1e-06)

    @pl.when(pl.program_id(0) == 0)
    def _():
        units[...] = jnp.zeros(units.shape, units.dtype)
        units[:rank, :v_cols] = rows[:, :v_cols]
        units[rank:, v_cols:] = rows[:, v_cols:cols]
        step = scale * jnp.dot(
            own[:, : 2 * rank], units[...], preferred_element_type=jnp.float32
        )
        step_v[...] = step[:, :v_cols]
        step_q[...] = step[:, v_cols:]
        new_v[...] = v_weight[...] - learn_rate * step[:, :v_cols]
        new_q[...] = q_weight[...] - learn_rate * step[:, v_cols:]

    step = jnp.dot(parcels[:, : 2 * rank], units[...], preferred_element_type=jnp.float32)
    new = parcels[:, 2 * rank :].astype(jnp.float32) - (learn_rate * scale) * step
    copy_v[...] = new[:, :v_cols].astype(jnp.bfloat16)
    copy_q[...] = new[:, v_cols:].T.astype(jnp.bfloat16)


def on_device(
    inputs,
    query_cot,
    value_cot,
    query_factor,
    value_factor,
    query_weight,
    value_weight,
    query_first,
    query_second,
    value_first,
    value_second,
):
    sizes = tuple(lax.axis_size(a) for a in FS)
    n0, n1, n2 = sizes
    tp = lax.axis_size("tp")
    own, rank = query_factor.shape
    q_cols = query_cot.shape[1]
    v_cols = value_cot.shape[1]
    cols = q_cols + v_cols
    width = rank // tp
    whole = rank * own
    bf16, f32 = jnp.bfloat16, jnp.float32
    shape = jax.ShapeDtypeStruct
    vmem = pl.BlockSpec(memory_space=pltpu.VMEM)
    smem = pl.BlockSpec(memory_space=pltpu.SMEM)
    at = lax.axis_index("tp").astype(jnp.int32).reshape(1)

    parcel, spread = pl.pallas_call(
        lambda *refs: pack_kernel(*refs, sizes=sizes, width=width),
        in_specs=[smem] + [vmem] * 4,
        out_specs=[vmem] * 2,
        out_shape=[shape((own, 2 * rank + cols), bf16), shape((n0, own, 2 * width), bf16)],
        name="pack",
    )(at, value_factor, query_factor, value_weight, query_weight)
    parcels = lax.all_gather(parcel, FS, axis=0, tiled=True)

    near = lax.all_to_all(spread, "fs_0", 0, 0, tiled=True)
    near = sent_to_all(near, "fs_1")
    near = sent_to_all(near, "fs_2")
    share = near.transpose(2, 1, 0, 3, 4).reshape(-1, 2 * width)
    proj = lax.dot_general(
        share, inputs, (((0,), (1,)), ((), ())), preferred_element_type=f32
    ).astype(bf16)
    proj = lax.all_gather(proj, "tp", axis=0, tiled=True).reshape(tp, 2, width, -1)
    proj_v = proj[:, 0].reshape(rank, -1)
    proj_q = proj[:, 1].reshape(rank, -1)

    term_v = jnp.dot(proj_v, value_cot, preferred_element_type=f32)
    term_q = jnp.dot(proj_q, query_cot, preferred_element_type=f32)
    term = jnp.concatenate([term_v, term_q], axis=1)
    term = summed_share(term, "fs_2")
    term = summed_share(term, "fs_0")
    term = lax.all_to_all(term.reshape(n1, 1, cols), "fs_1", 0, 0, tiled=True)
    first_v, second_v, first_q, second_q, spread = pl.pallas_call(
        moments_kernel,
        in_specs=[vmem] * 5,
        out_specs=[vmem] * 5,
        out_shape=[shape((1, v_cols), f32)] * 2
        + [shape((1, q_cols), f32)] * 2
        + [shape((n1 * tp, 8, 128), bf16)],
        name="moments",
    )(term, value_first, value_second, query_first, query_second)

    blocks = lax.all_to_all(spread, ("fs_1", "tp"), 0, 0, tiled=True)
    lines = -(-(cols + 3) // 128)
    spread = pl.pallas_call(
        lambda *refs: regroup_kernel(*refs, cols=cols),
        in_specs=[smem, vmem],
        out_specs=vmem,
        out_shape=shape((n0, n1, lines * 128), bf16),
        name="regroup",
    )(at, blocks.reshape(n1, tp, 8, 128))
    rows = lax.all_to_all(spread, "fs_0", 0, 0, tiled=True).reshape(n0 * n1, -1)
    rows = sent_to_all(rows, "fs_2").reshape(rank, -1)

    steps = 8
    block = whole // steps
    fixed = lambda *s: pl.BlockSpec(s, lambda i: (0, 0))
    step_v, step_q, new_v, new_q, copy_v, copy_q = pl.pallas_call(
        lambda *refs: update_kernel(
            *refs, rank=rank, v_cols=v_cols, q_cols=q_cols, entries=rank * cols * tp
        ),
        grid=(steps,),
        in_specs=[
            fixed(rank, lines * 128),
            fixed(own, 2 * rank + cols),
            fixed(own, v_cols),
            fixed(own, q_cols),
            pl.BlockSpec((block, 2 * rank + cols), lambda i: (i, 0)),
        ],
        out_specs=[
            fixed(own, v_cols),
            fixed(own, q_cols),
            fixed(own, v_cols),
            fixed(own, q_cols),
            pl.BlockSpec((block, v_cols), lambda i: (i, 0)),
            pl.BlockSpec((q_cols, block), lambda i: (0, i)),
        ],
        out_shape=[
            shape((own, v_cols), f32),
            shape((own, q_cols), f32),
            shape((own, v_cols), f32),
            shape((own, q_cols), f32),
            shape((whole, v_cols), bf16),
            shape((q_cols, whole), bf16),
        ],
        scratch_shapes=[pltpu.VMEM((2 * rank, cols), bf16)],
        name="update",
    )(rows, parcel, value_weight, query_weight, parcels)
    return (step_q, step_v, new_q, new_v, first_q, second_q, first_v, second_v, copy_q.T, copy_v)


def solution(mesh):
    split = Mesh(mesh.devices.reshape(12, 8, 2, mesh.shape["tp"]), ("fs_0", "fs_1", "fs_2", "tp"))
    return jax.shard_map(
        on_device,
        mesh=split,
        in_specs=(
            P(FS, None),
            P(FS, "tp"),
            P(FS, "tp"),
            P(FS, None),
            P(FS, None),
            P(FS, "tp"),
            P(FS, "tp"),
            P(FS, "tp"),
            P(FS, "tp"),
            P(FS, "tp"),
            P(FS, "tp"),
        ),
        out_specs=(
            P(FS, "tp"),
            P(FS, "tp"),
            P(FS, "tp"),
            P(FS, "tp"),
            P(FS, "tp"),
            P(FS, "tp"),
            P(FS, "tp"),
            P(FS, "tp"),
            P(None, "tp"),
            P(None, "tp"),
        ),
        check_vma=False,
    )
```

time: 312 us -> 168 us (0.54)
  waiting for transfers between devices: 152 us -> 0.02 us
  blocking collectives: 79.4 us -> 136 us
  local copies, waits for them, and re-layouts: 22.1 us -> 0.52 us
  starting transfers between devices: 16 us -> 0.04 us
  Pallas kernels: 0 us -> 14.1 us
  matrix products: 12.2 us -> 2.74 us
  other arithmetic: 8.87 us -> 0.09 us
  between operations: 20.5 us -> 14.2 us
    all_gather x1, waiting for transfers between devices: 112 us -> 0.01 us  [on_device(): parcels = lax.all_gather(parcel, FS, axis=0, tiled=True)]
    all_to_all x0 -> x4, blocking collectives: none -> 64.6 us  [the longest x1 25.7 us: on_device(): near = lax.all_to_all(spread, 'fs_0', 0, 0, tiled=True)]
    all_to_all x4 -> x0, waiting for transfers between devices: 39.7 us -> none  [the longest x2 20.7 us: summed_share(): return lax.all_to_all(parts, axis, 0, 0, tiled=True).sum(axis=0)]
    all_to_all x4 -> x3, blocking collectives: 61.3 us -> 36 us  [sent_to_all(): lax.all_to_all(jnp.broadcast_to(value[None], (size, *value.shape)), axis,...]
    all_to_all x1 -> x2, blocking collectives: 5.99 us -> 23 us  [summed_share(): return lax.all_to_all(parts, axis, 0, 0, tiled=True).sum(axis=0)]
    all_to_all x4 -> x0, starting transfers between devices: 15.9 us -> none  [the longest x2 9.04 us: sent_to_all(): lax.all_to_all(jnp.broadcast_to(value[None], (size, *value.shape)), axis,...]
    pallas_call x0 -> x4, Pallas kernels: none -> 14.1 us  [the longest x1 9.28 us: on_device(): pl.pallas_call(lambda *refs: update_kernel(*refs, rank=rank, v_cols=v_col...]
    unnamed x27 -> x6, local copies, waits for them, and re-layouts: 13.2 us -> 0.02 us
  transfers between devices with their start and end apart: 5 -> 1, of which waited for: 5 -> 0; matrix products, arithmetic and copies ran while one was open for 0% -> 2% of each run, Pallas kernels for 0% -> 2%
where the time goes in v2:
time: 168 us; the launch traced here: 167 us
  blocking collectives  136 us (81%)
  between operations  14.2 us (8%)
  Pallas kernels  14.1 us (8%)
  matrix products  2.74 us (2%)
    all_to_all x3, blocking collectives, sent_to_all(): lax.all_to_all(jnp.broadcast_to(value[None], (size, *value.shape)), axis,...  36 us
    all_to_all x1, blocking collectives, on_device(): near = lax.all_to_all(spread, 'fs_0', 0, 0, tiled=True)  25.7 us
    all_to_all x2, blocking collectives, summed_share(): return lax.all_to_all(parts, axis, 0, 0, tiled=True).sum(axis=0)  23 us
    all_to_all x1, blocking collectives, on_device(): rows = lax.all_to_all(spread, 'fs_0', 0, 0, tiled=True).reshape(n0 * n1, -1)  15 us
    all_to_all x1, blocking collectives, on_device(): blocks = lax.all_to_all(spread, ('fs_1', 'tp'), 0, 0, tiled=True)  14.2 us
    all_gather x1, blocking collectives, on_device(): lax.all_gather(proj, 'tp', axis=0, tiled=True).reshape(tp, 2, width, -1)  12 us
    all_to_all x1, blocking collectives, on_device(): term = lax.all_to_all(term.reshape(n1, 1, cols), 'fs_1', 0, 0, tiled=True)  9.73 us
    pallas_call x1, Pallas kernels, on_device(): pl.pallas_call(lambda *refs: update_kernel(*refs, rank=rank, v_cols=v_col...  9.28 us
  transfers between devices with their start and end apart: 1, of which 0 were waited for; matrix products, arithmetic and copies ran while one was open for 2% of the time, Pallas kernels for 2%

profile of v2, /device:TPU:1, one launch (start us, length us, event | category | flops | bytes accessed | tf_op | source)
XLA Modules:
  0.0 167.3 jit_solution(14008418318868049086)
XLA Ops:
  7.2 0.0 copy-start
  7.2 0.0 all-gather.2.cloned.1.call-start
  7.2 1.7 %pack.1 = (bf16[16,960]{1,0:T(8,128)(2,1)}, bf16[12,16,96]{2,1,0:T(8,128)(2,1)}) custom-call(s32[1]{0:T(128)} %bitcast.refs_0_, bf16[16,192]{1,0:T(8,128)(2,1)} %refs_1_.1, bf16[16,192]{1,0:T(8,128)(2,1)} %refs_2_.2, f32[16,384]{1,0:T(8,128)} %refs_2_.3, f32[16,192]{1,0:T(8,128)} %refs_3_.3), custom_call_target="tpu_custom_call" | custom-call | tf_op jit(solution)/shard_map/pack/pallas_call | solution.py:185
  9.0 0.0 all-gather.2.cloned.1.call-update
  9.0 0.0 copy-start.1
  9.0 25.7 %all_to_all.45 = bf16[12,16,96]{2,1,0:T(8,128)(2,1)S(1)} all-to-all(bf16[12,16,96]{2,1,0:T(8,128)(2,1)} %get-tuple-element.23), channel_id=1, replica_groups=mesh['fs_0'=12,'fs_1'=8,'fs_2'=2,'tp'=4] {'fs_0'}, dimensions={0} | all-to-all | bytes 73728 | tf_op jit(solution)/shard_map/all_to_all | solution.py:194
  34.6 0.1 broadcast_in_dim.8
  34.7 18.6 %all_to_all.46 = bf16[8,12,16,96]{3,2,1,0:T(8,128)(2,1)S(1)} all-to-all(bf16[8,12,16,96]{3,2,1,0:T(8,128)(2,1)S(1)} %broadcast_in_dim.8), channel_id=1, replica_groups=mesh['fs_0'=12,'fs_1'=8,'fs_2'=2,'tp'=4] {'fs_1'}, dimensions={0} | all-to-all | bytes 589824 | tf_op jit(solution)/shard_map/all_to_all | solution.py:22
  53.3 0.2 broadcast_in_dim.9
  53.5 0.0 copy-start.2
  53.5 8.1 %all_to_all.47 = bf16[2,8,12,16,96]{4,3,1,2,0:T(8,128)(2,1)S(1)} all-to-all(bf16[2,8,12,16,96]{4,3,1,2,0:T(8,128)(2,1)S(1)} %broadcast_in_dim.9), channel_id=1, replica_groups=mesh['fs_0'=12,'fs_1'=8,'fs_2'=2,'tp'=4] {'fs_2'}, dimensions={0} | all-to-all | bytes 1179648 | tf_op jit(solution)/shard_map/all_to_all | solution.py:22
  61.7 0.1 copy.24
  61.8 0.0 copy-done.1
  61.8 2.1 %convolution_convert_fusion = bf16[96,1024]{1,0:T(8,128)(2,1)S(1)} fusion(bf16[3072,96]{1,0:T(8,128)(2,1)S(1)} %bitcast.18, bf16[1024,3072]{1,0:T(8,128)(2,1)S(1)} %copy-done.1), kind=kOutput, calls=%fused_computation | convolution fusion | flops 604078080 | bytes 7077888 | tf_op jit(solution)/shard_map/dot_general | solution.py:198
  63.9 12.0 %all_gather.6 = bf16[384,1024]{1,0:T(8,128)(2,1)S(1)} all-gather(bf16[96,1024]{1,0:T(8,128)(2,1)S(1)} %convolution_convert_fusion), channel_id=1, replica_groups=mesh['fs_0'=12,'fs_1'=8,'fs_2'=2,'tp'=4] {'tp'}, dimensions={0}, use_global_device_ids=true | all-gather | bytes 983040 | tf_op jit(solution)/shard_map/all_gather | solution.py:201
  75.9 0.1 fusion
  76.0 0.0 copy-done.2
  76.0 0.3 fusion.2
  76.3 0.0 copy-done
  76.3 0.4 fusion.1
  76.7 6.0 %all_to_all.48 = f32[2,96,576]{2,1,0:T(8,128)S(1)} all-to-all(f32[2,96,576]{2,1,0:T(8,128)S(1)} %bitcast.21), channel_id=1, replica_groups=mesh['fs_0'=12,'fs_1'=8,'fs_2'=2,'tp'=4] {'fs_2'}, dimensions={0} | all-to-all | bytes 884736 | tf_op jit(solution)/shard_map/all_to_all | solution.py:30
  82.7 17.0 %all_to_all.49 = f32[12,8,576]{2,1,0:T(8,128)S(1)} all-to-all(f32[12,8,576]{2,1,0:T(8,128)S(1)} %bitcast.25), channel_id=1, replica_groups=mesh['fs_0'=12,'fs_1'=8,'fs_2'=2,'tp'=4] {'fs_0'}, dimensions={0} | all-to-all | bytes 442368 | tf_op jit(solution)/shard_map/all_to_all | solution.py:30
  99.8 9.7 %all_to_all.50.terms = f32[8,1,576]{2,1,0:T(1,128)} all-to-all(f32[8,1,576]{2,1,0:T(1,128)S(1)} %reshape.52), channel_id=1, replica_groups=mesh['fs_0'=12,'fs_1'=8,'fs_2'=2,'tp'=4] {'fs_1'}, dimensions={0} | all-to-all | bytes 36864 | tf_op jit(solution)/shard_map/all_to_all | solution.py:210
  109.6 1.6 moments.1
  111.1 14.2 %all_to_all.51 = bf16[32,8,128]{2,1,0:T(8,128)(2,1)} all-to-all(bf16[32,8,128]{2,1,0:T(8,128)(2,1)} %get-tuple-element.24), channel_id=1, replica_groups=mesh['fs_0'=12,'fs_1'=8,'fs_2'=2,'tp'=4] {'fs_1','tp'}, dimensions={0} | all-to-all | bytes 131072 | tf_op jit(solution)/shard_map/all_to_all | solution.py:221
  125.3 1.6 regroup.1
  126.9 15.0 %all_to_all.52 = bf16[12,8,640]{2,1,0:T(8,128)(2,1)S(1)} all-to-all(bf16[12,8,640]{2,1,0:T(8,128)(2,1)} %regroup.1), channel_id=1, replica_groups=mesh['fs_0'=12,'fs_1'=8,'fs_2'=2,'tp'=4] {'fs_0'}, dimensions={0} | all-to-all | bytes 245760 | tf_op jit(solution)/shard_map/all_to_all | solution.py:230
  141.9 9.2 %all_to_all.53 = bf16[2,96,640]{2,1,0:T(8,128)(2,1)} all-to-all(bf16[2,96,640]{2,1,0:T(8,128)(2,1)S(1)} %broadcast_in_dim.22), channel_id=1, replica_groups=mesh['fs_0'=12,'fs_1'=8,'fs_2'=2,'tp'=4] {'fs_2'}, dimensions={0} | all-to-all | bytes 491520 | tf_op jit(solution)/shard_map/all_to_all | solution.py:22
  151.1 0.0 all-gather.2.cloned.1.call-done.refs_4_
  151.1 9.3 %update.1 = (f32[16,384]{1,0:T(8,128)}, f32[16,192]{1,0:T(8,128)}, f32[16,384]{1,0:T(8,128)}, f32[16,192]{1,0:T(8,128)}, bf16[3072,384]{1,0:T(8,128)(2,1)}, /*index=5*/bf16[192,3072]{1,0:T(8,128)(2,1)}) custom-call(bf16[192,640]{1,0:T(8,128)(2,1)} %bitcast.24, bf16[16,960]{1,0:T(8,128)(2,1)} %get-tuple-element.25.refs_1_, f32[16,384]{1,0:T(8,128)} %refs_2_.3, ...), custom_call_target="tpu_custom_call" | custom-call | tf_op jit(solution)/shard_map/update/pallas_call | solution.py:236
  (6 shorter events, 0.1 us)
Async XLA Ops:
  7.2 69.1 %copy-start = (bf16[1024,384]{1,0:T(8,128)(2,1)S(1)}, bf16[1024,384]{1,0:T(8,128)(2,1)}, u32[]{:S(2)}) copy-start(bf16[1024,384]{1,0:T(8,128)(2,1)} %param.13) | copy-start | bytes 2359300
  7.2 143.9 %all-gather.2.cloned.1.call-start = ((), (), s32[]{:S(2)}) async-start(), calls=%async_computation.9 | async-start | bytes 6324224 | tf_op jit(solution)/shard_map/all_gather | solution.py:192
  9.0 52.9 %copy-start.1 = (bf16[1024,3072]{1,0:T(8,128)(2,1)S(1)}, bf16[1024,3072]{1,0:T(8,128)(2,1)}, u32[]{:S(2)}) copy-start(bf16[1024,3072]{1,0:T(8,128)(2,1)} %param.11) | copy-start | bytes 18874372
  53.5 22.5 %copy-start.2 = (bf16[1024,192]{0,1:T(8,128)(2,1)S(1)}, bf16[1024,192]{0,1:T(8,128)(2,1)}, u32[]{:S(2)}) copy-start(bf16[1024,192]{0,1:T(8,128)(2,1)} %param.12) | copy-start | bytes 1179652
Sparse Core Ops, SparseCore 0:
  11.8 132.9 all-gather.1

commit v3 on v2

--- a/solution.py
+++ b/solution.py
@@ -24,12 +24,6 @@
     )
 
 
-def summed_share(value, axis):
-    size = lax.axis_size(axis)
-    parts = value.reshape(size, -1, *value.shape[1:])
-    return lax.all_to_all(parts, axis, 0, 0, tiled=True).sum(axis=0)
-
-
 def shift_of(size):
     shift = int(math.log2(size))
     assert 1 << shift == size
@@ -40,13 +34,11 @@
     own, rank = v_factor.shape
     n0, n1, n2 = sizes
     row = lax.broadcasted_iota(jnp.int32, (rank, rank), 0)
-    place = (
-        (row & (n2 - 1)) * (n0 * n1)
-        + (row >> shift_of(n1 * n2)) * n1
-        + ((row >> shift_of(n2)) & (n1 - 1))
-    )
+    far = row >> shift_of(n1 * n2)
+    place = (row & (n2 - 1)) * (n0 * n1) + far * n1 + ((row >> shift_of(n2)) & (n1 - 1))
     col = lax.broadcasted_iota(jnp.int32, (rank, rank), 1)
     turn = (place == col).astype(jnp.float32).astype(jnp.bfloat16)
+    place = (row & (n1 * n2 - 1)) * n0 + far
     mine = (place == col + at[0] * width) & (col < width)
     mine = mine.astype(jnp.float32).astype(jnp.bfloat16)
 
@@ -67,6 +59,46 @@
     spread[...] = jnp.broadcast_to(share[None], spread.shape)
 
 
+def terms_kernel(proj, v_cot, q_cot, blocks, term_v, term_q, wide, *, n0, width):
+    rank, v_cols = term_v.shape
+    tp = rank // width
+    parts = [proj[2 * width * t : 2 * width * (t + 1), :] for t in range(tp)]
+    proj_v = jnp.concatenate([p[:width] for p in parts], axis=0)
+    proj_q = jnp.concatenate([p[width:] for p in parts], axis=0)
+    term_v[...] = jnp.dot(proj_v, v_cot[...], preferred_element_type=jnp.float32)
+    term_q[...] = lax.dot_general(
+        proj_q, q_cot[...], (((1,), (1,)), ((), ())), preferred_element_type=jnp.float32
+    )
+    chunks, half = v_cols // 128, n0 // 2
+    wide[...] = jnp.zeros(wide.shape, jnp.float32)
+    for b in range(rank // n0):
+        for k in range(chunks):
+            wide[b, n0 * k : n0 * (k + 1), :] = term_v[
+                n0 * b : n0 * (b + 1), 128 * k : 128 * (k + 1)
+            ]
+        wide[b, n0 * chunks : n0 * (chunks + 1), :] = term_q[n0 * b : n0 * (b + 1), :128]
+        rest = jnp.concatenate(
+            [term_q[n0 * b : n0 * b + half, 128:], term_q[n0 * b + half : n0 * (b + 1), 128:]],
+            axis=1,
+        )
+        wide[b, n0 * (chunks + 1) : n0 * (chunks + 1) + half, :] = rest
+    blocks[...] = wide[...].astype(jnp.bfloat16)
+
+
+def fold_kernel(blocks, rows, wide, *, n0, chunks):
+    wide[...] = jnp.sum(blocks[...].astype(jnp.float32), axis=0)
+    half = n0 // 2
+    rows[...] = jnp.zeros(rows.shape, jnp.float32)
+    for r in range(n0):
+        for k in range(chunks + 1):
+            rows[r, k : k + 1, :] = wide[n0 * k + r : n0 * k + r + 1, :]
+        line = n0 * (chunks + 1) + r % half
+        rest = wide[line : line + 1, :]
+        if r >= half:
+            rest = jnp.concatenate([rest[:, 64:], rest[:, :64]], axis=1)
+        rows[r, chunks + 1 : chunks + 2, :] = rest
+
+
 def pieces_of(value):
     high = value.astype(jnp.bfloat16).astype(jnp.float32)
     middle = (value - high).astype(jnp.bfloat16).astype(jnp.float32)
@@ -89,8 +121,13 @@
 
 def moments_kernel(terms, v_first, v_second, q_first, q_second, *outs):
     first_v, second_v, first_q, second_q, spread = outs
-    v_cols = v_first.shape[1]
+    v_cols, q_cols = v_first.shape[1], q_first.shape[1]
     gradient = jnp.sum(terms[...], axis=0)
+    gradient = jnp.concatenate(
+        [gradient[k : k + 1] for k in range(v_cols // 128 + 1)]
+        + [gradient[v_cols // 128 + 1 : v_cols // 128 + 2, : q_cols - 128]],
+        axis=1,
+    )
     first_v[...], second_v[...], unit_v = moments(v_first[...], v_second[...], gradient[:, :v_cols])
     first_q[...], second_q[...], unit_q = moments(q_first[...], q_second[...], gradient[:, v_cols:])
     squares = jnp.sum(unit_v * unit_v, axis=1, keepdims=True)
@@ -127,18 +164,20 @@
 
 def update_kernel(
     rows, own, v_weight, q_weight, parcels, step_v, step_q, new_v, new_q, copy_v, copy_q, units,
-    *, rank, v_cols, q_cols, entries
+    rate, *, rank, v_cols, q_cols, entries
 ):
     cols = v_cols + q_cols
-    tail = rows[:, cols // 128 * 128 :].astype(jnp.float32)
-    lane = lax.broadcasted_iota(jnp.int32, tail.shape, 1) + cols // 128 * 128
-    total = jnp.sum(jnp.where((lane >= cols) & (lane < cols + 3), tail, 0.0), keepdims=True)
-    scale = lax.rsqrt(total / entries + 1e-06)
 
     @pl.when(pl.program_id(0) == 0)
     def _():
-        units[...] = jnp.zeros(units.shape, units.dtype)
+        tail = rows[:, cols // 128 * 128 :].astype(jnp.float32)
+        lane = lax.broadcasted_iota(jnp.int32, tail.shape, 1) + cols // 128 * 128
+        total = jnp.sum(jnp.where((lane >= cols) & (lane < cols + 3), tail, 0.0), keepdims=True)
+        scale = lax.rsqrt(total / entries + 1e-06)
+        rate[...] = jnp.broadcast_to(learn_rate * scale, rate.shape)
         units[:rank, :v_cols] = rows[:, :v_cols]
+        units[rank:, :v_cols] = jnp.zeros((rank, v_cols), units.dtype)
+        units[:rank, v_cols:] = jnp.zeros((rank, q_cols), units.dtype)
         units[rank:, v_cols:] = rows[:, v_cols:cols]
         step = scale * jnp.dot(
             own[:, : 2 * rank], units[...], preferred_element_type=jnp.float32
@@ -148,10 +187,14 @@
         new_v[...] = v_weight[...] - learn_rate * step[:, :v_cols]
         new_q[...] = q_weight[...] - learn_rate * step[:, v_cols:]
 
-    step = jnp.dot(parcels[:, : 2 * rank], units[...], preferred_element_type=jnp.float32)
-    new = parcels[:, 2 * rank :].astype(jnp.float32) - (learn_rate * scale) * step
-    copy_v[...] = new[:, :v_cols].astype(jnp.bfloat16)
-    copy_q[...] = new[:, v_cols:].T.astype(jnp.bfloat16)
+    to_v, from_q = min(rank + -rank % 128, 2 * rank), rank // 128 * 128
+    weights = parcels[:, 2 * rank :].astype(jnp.float32)
+    step = jnp.dot(parcels[:, :to_v], units[:to_v, :v_cols], preferred_element_type=jnp.float32)
+    copy_v[...] = (weights[:, :v_cols] - rate[:, :v_cols] * step).astype(jnp.bfloat16)
+    step = jnp.dot(
+        parcels[:, from_q : 2 * rank], units[from_q:, v_cols:], preferred_element_type=jnp.float32
+    )
+    copy_q[...] = (weights[:, v_cols:] - rate[:, v_cols:] * step).astype(jnp.bfloat16).T
 
 
 def on_device(
@@ -180,13 +223,14 @@
     shape = jax.ShapeDtypeStruct
     vmem = pl.BlockSpec(memory_space=pltpu.VMEM)
     smem = pl.BlockSpec(memory_space=pltpu.SMEM)
+    near_core = lambda a: pltpu.with_memory_space_constraint(a, pltpu.VMEM)
     at = lax.axis_index("tp").astype(jnp.int32).reshape(1)
 
     parcel, spread = pl.pallas_call(
         lambda *refs: pack_kernel(*refs, sizes=sizes, width=width),
         in_specs=[smem] + [vmem] * 4,
         out_specs=[vmem] * 2,
-        out_shape=[shape((own, 2 * rank + cols), bf16), shape((n0, own, 2 * width), bf16)],
+        out_shape=[shape((own, 2 * rank + cols), bf16), pltpu.VMEM((n0, own, 2 * width), bf16)],
         name="pack",
     )(at, value_factor, query_factor, value_weight, query_weight)
     parcels = lax.all_gather(parcel, FS, axis=0, tiled=True)
@@ -198,25 +242,48 @@
     proj = lax.dot_general(
         share, inputs, (((0,), (1,)), ((), ())), preferred_element_type=f32
     ).astype(bf16)
-    proj = lax.all_gather(proj, "tp", axis=0, tiled=True).reshape(tp, 2, width, -1)
-    proj_v = proj[:, 0].reshape(rank, -1)
-    proj_q = proj[:, 1].reshape(rank, -1)
-
-    term_v = jnp.dot(proj_v, value_cot, preferred_element_type=f32)
-    term_q = jnp.dot(proj_q, query_cot, preferred_element_type=f32)
-    term = jnp.concatenate([term_v, term_q], axis=1)
-    term = summed_share(term, "fs_2")
-    term = summed_share(term, "fs_0")
-    term = lax.all_to_all(term.reshape(n1, 1, cols), "fs_1", 0, 0, tiled=True)
+    proj = lax.all_gather(proj, "tp", axis=0, tiled=True)
+
+    chunks = v_cols // 128
+    lines = n0 * (chunks + 1) + n0 // 2
+    lines += -lines % 8
+    blocks = pl.pallas_call(
+        lambda *refs: terms_kernel(*refs, n0=n0, width=width),
+        in_specs=[vmem] * 3,
+        out_specs=vmem,
+        out_shape=pltpu.VMEM((n1 * n2, lines, 128), bf16),
+        scratch_shapes=[
+            pltpu.VMEM((rank, v_cols), f32),
+            pltpu.VMEM((rank, q_cols), f32),
+            pltpu.VMEM((n1 * n2, lines, 128), f32),
+        ],
+        name="terms",
+    )(near_core(proj), near_core(value_cot), near_core(query_cot.T))
+    blocks = lax.all_to_all(blocks, ("fs_1", "fs_2"), 0, 0, tiled=True)
+    term = pl.pallas_call(
+        lambda *refs: fold_kernel(*refs, n0=n0, chunks=chunks),
+        in_specs=[vmem],
+        out_specs=vmem,
+        out_shape=pltpu.VMEM((n0, 8, 128), f32),
+        scratch_shapes=[pltpu.VMEM((lines, 128), f32)],
+        name="fold",
+    )(near_core(blocks))
+    term = lax.all_to_all(term, "fs_0", 0, 0, tiled=True)
     first_v, second_v, first_q, second_q, spread = pl.pallas_call(
         moments_kernel,
         in_specs=[vmem] * 5,
         out_specs=[vmem] * 5,
         out_shape=[shape((1, v_cols), f32)] * 2
         + [shape((1, q_cols), f32)] * 2
-        + [shape((n1 * tp, 8, 128), bf16)],
+        + [pltpu.VMEM((n1 * tp, 8, 128), bf16)],
         name="moments",
-    )(term, value_first, value_second, query_first, query_second)
+    )(
+        near_core(term),
+        near_core(value_first),
+        near_core(value_second),
+        near_core(query_first),
+        near_core(query_second),
+    )
 
     blocks = lax.all_to_all(spread, ("fs_1", "tp"), 0, 0, tiled=True)
     lines = -(-(cols + 3) // 128)
@@ -224,13 +291,13 @@
         lambda *refs: regroup_kernel(*refs, cols=cols),
         in_specs=[smem, vmem],
         out_specs=vmem,
-        out_shape=shape((n0, n1, lines * 128), bf16),
+        out_shape=pltpu.VMEM((n0, n1, lines * 128), bf16),
         name="regroup",
-    )(at, blocks.reshape(n1, tp, 8, 128))
+    )(at, near_core(blocks.reshape(n1, tp, 8, 128)))
     rows = lax.all_to_all(spread, "fs_0", 0, 0, tiled=True).reshape(n0 * n1, -1)
     rows = sent_to_all(rows, "fs_2").reshape(rank, -1)
 
-    steps = 8
+    steps = 2
     block = whole // steps
     fixed = lambda *s: pl.BlockSpec(s, lambda i: (0, 0))
     step_v, step_q, new_v, new_q, copy_v, copy_q = pl.pallas_call(
@@ -261,9 +328,9 @@
             shape((whole, v_cols), bf16),
             shape((q_cols, whole), bf16),
         ],
-        scratch_shapes=[pltpu.VMEM((2 * rank, cols), bf16)],
+        scratch_shapes=[pltpu.VMEM((2 * rank, cols), bf16), pltpu.VMEM((1, cols), f32)],
         name="update",
-    )(rows, parcel, value_weight, query_weight, parcels)
+    )(near_core(rows), parcel, value_weight, query_weight, parcels)
     return (step_q, step_v, new_q, new_v, first_q, second_q, first_v, second_v, copy_q.T, copy_v)
 
 

time: 168 us -> 158 us (0.940)
  blocking collectives: 136 us -> 128 us
  Pallas kernels: 14.1 us -> 8.01 us
  waiting for transfers between devices: 0.02 us -> 4.9 us
    all_to_all x3 -> x2, blocking collectives: 32.8 us -> 27.6 us  [the longest x1 15.4 us: on_device(): blocks = lax.all_to_all(blocks, ('fs_1', 'fs_2'), 0, 0, tiled=True)]
    all_gather x1, waiting for transfers between devices: 0.01 us -> 4.88 us  [on_device(): parcels = lax.all_gather(parcel, FS, axis=0, tiled=True)]
    pallas_call x1, Pallas kernels: 9.28 us -> 5 us  [on_device(): pl.pallas_call(lambda *refs: update_kernel(*refs, rank=rank, v_cols=v_col...]
    all_to_all x3, blocking collectives: 36 us -> 33.3 us  [sent_to_all(): lax.all_to_all(jnp.broadcast_to(value[None], (size, *value.shape)), axis,...]
  transfers between devices with their start and end apart: 1 -> 1, of which waited for: 0 -> 1; matrix products, arithmetic and copies ran while one was open for 2% -> 2% of each run, Pallas kernels for 2% -> 1%
where the time goes in v3:
time: 158 us; the launch traced here: 157 us
  blocking collectives  128 us (81%)
  between operations  14.1 us (9%)
  Pallas kernels  8.01 us (5%)
  waiting for transfers between devices  4.9 us (3%)
  matrix products  2.09 us (1%)
    all_to_all x3, blocking collectives, sent_to_all(): lax.all_to_all(jnp.broadcast_to(value[None], (size, *value.shape)), axis,...  33.3 us
    all_to_all x1, blocking collectives, on_device(): near = lax.all_to_all(spread, 'fs_0', 0, 0, tiled=True)  25.4 us
    all_to_all x1, blocking collectives, on_device(): blocks = lax.all_to_all(blocks, ('fs_1', 'fs_2'), 0, 0, tiled=True)  15.4 us
    all_to_all x1, blocking collectives, on_device(): rows = lax.all_to_all(spread, 'fs_0', 0, 0, tiled=True).reshape(n0 * n1, -1)  14.7 us
    all_to_all x1, blocking collectives, on_device(): blocks = lax.all_to_all(spread, ('fs_1', 'tp'), 0, 0, tiled=True)  14.3 us
    all_gather x1, blocking collectives, on_device(): proj = lax.all_gather(proj, 'tp', axis=0, tiled=True)  12.3 us
    all_to_all x1, blocking collectives, on_device(): term = lax.all_to_all(term, 'fs_0', 0, 0, tiled=True)  12.2 us
    pallas_call x1, Pallas kernels, on_device(): pl.pallas_call(lambda *refs: update_kernel(*refs, rank=rank, v_cols=v_col...  5 us
  transfers between devices with their start and end apart: 1, of which 1 were waited for; matrix products, arithmetic and copies ran while one was open for 2% of the time, Pallas kernels for 1%

profile of v3, /device:TPU:1, one launch (start us, length us, event | category | flops | bytes accessed | tf_op | source)
XLA Modules:
  0.0 157.4 jit_solution(10372420222029613903)
XLA Ops:
  7.2 0.0 all-gather.2.cloned.1.call-start
  7.2 1.6 %pack.1 = (bf16[16,960]{1,0:T(8,128)(2,1)}, bf16[12,16,96]{2,1,0:T(8,128)(2,1)S(1)}) custom-call(s32[1]{0:T(128)} %bitcast.refs_0_, bf16[16,192]{1,0:T(8,128)(2,1)} %refs_1_.2, bf16[16,192]{1,0:T(8,128)(2,1)} %refs_2_.2, f32[16,384]{1,0:T(8,128)} %refs_2_.3, f32[16,192]{1,0:T(8,128)} %refs_3_.3), custom_call_target="tpu_custom_call" | custom-call | tf_op jit(solution)/shard_map/pack/pallas_call | solution.py:229
  8.8 0.0 all-gather.2.cloned.1.call-update
  8.9 0.0 copy-start.6
  8.9 25.4 %all_to_all.40 = bf16[12,16,96]{2,1,0:T(8,128)(2,1)S(1)} all-to-all(bf16[12,16,96]{2,1,0:T(8,128)(2,1)S(1)} %get-tuple-element.23), channel_id=1, replica_groups=mesh['fs_0'=12,'fs_1'=8,'fs_2'=2,'tp'=4] {'fs_0'}, dimensions={0} | all-to-all | bytes 73728 | tf_op jit(solution)/shard_map/all_to_all | solution.py:238
  34.3 0.1 broadcast_in_dim.8
  34.4 18.6 %all_to_all.41 = bf16[8,12,16,96]{3,2,1,0:T(8,128)(2,1)S(1)} all-to-all(bf16[8,12,16,96]{3,2,1,0:T(8,128)(2,1)S(1)} %broadcast_in_dim.8), channel_id=1, replica_groups=mesh['fs_0'=12,'fs_1'=8,'fs_2'=2,'tp'=4] {'fs_1'}, dimensions={0} | all-to-all | bytes 589824 | tf_op jit(solution)/shard_map/all_to_all | solution.py:22
  53.0 0.0 copy-start
  53.0 0.0 copy-start.1
  53.1 0.2 broadcast_in_dim.9
  53.2 8.1 %all_to_all.42 = bf16[2,8,12,16,96]{4,3,1,2,0:T(8,128)(2,1)S(1)} all-to-all(bf16[2,8,12,16,96]{4,3,1,2,0:T(8,128)(2,1)S(1)} %broadcast_in_dim.9), channel_id=1, replica_groups=mesh['fs_0'=12,'fs_1'=8,'fs_2'=2,'tp'=4] {'fs_2'}, dimensions={0} | all-to-all | bytes 1179648 | tf_op jit(solution)/shard_map/all_to_all | solution.py:22
  61.4 0.0 copy-start.2
  61.4 0.0 copy-start.3
  61.4 0.0 copy-start.4
  61.4 0.0 copy-start.5
  61.4 0.1 copy.22
  61.5 0.0 copy-done.6
  61.5 2.1 %convolution_convert_fusion = bf16[96,1024]{1,0:T(8,128)(2,1)S(1)} fusion(bf16[3072,96]{1,0:T(8,128)(2,1)S(1)} %bitcast.13, bf16[1024,3072]{1,0:T(8,128)(2,1)S(1)} %copy-done.6), kind=kOutput, calls=%fused_computation | convolution fusion | flops 604078080 | bytes 7077888 | tf_op jit(solution)/shard_map/dot_general | solution.py:242
  63.6 12.3 %all_gather.6.refs_0_ = bf16[384,1024]{1,0:T(8,128)(2,1)S(1)} all-gather(bf16[96,1024]{1,0:T(8,128)(2,1)S(1)} %convolution_convert_fusion), channel_id=1, replica_groups=mesh['fs_0'=12,'fs_1'=8,'fs_2'=2,'tp'=4] {'tp'}, dimensions={0}, use_global_device_ids=true | all-gather | bytes 983040 | tf_op jit(solution)/shard_map/all_gather | solution.py:245
  75.9 0.0 copy-done
  75.9 0.0 copy-done.1
  75.9 0.6 terms.1
  76.5 15.4 %all_to_all.43.refs_0_ = bf16[16,56,128]{2,1,0:T(8,128)(2,1)S(1)} all-to-all(bf16[16,56,128]{2,1,0:T(8,128)(2,1)S(1)} %terms.1), channel_id=1, replica_groups=mesh['fs_0'=12,'fs_1'=8,'fs_2'=2,'tp'=4] {'fs_1','fs_2'}, dimensions={0} | all-to-all | bytes 458752 | tf_op jit(solution)/shard_map/all_to_all | solution.py:262
  91.9 0.1 fold.1
  92.0 12.2 %all_to_all.44.terms = f32[12,8,128]{2,1,0:T(8,128)S(1)} all-to-all(f32[12,8,128]{2,1,0:T(8,128)S(1)} %fold.1), channel_id=1, replica_groups=mesh['fs_0'=12,'fs_1'=8,'fs_2'=2,'tp'=4] {'fs_0'}, dimensions={0} | all-to-all | bytes 98304 | tf_op jit(solution)/shard_map/all_to_all | solution.py:271
  104.2 0.0 copy-done.2
  104.2 0.0 copy-done.3
  104.2 0.0 copy-done.4
  104.3 0.0 copy-done.5
  104.3 0.6 moments.1
  104.9 14.3 %all_to_all.45 = bf16[32,8,128]{2,1,0:T(8,128)(2,1)S(1)} all-to-all(bf16[32,8,128]{2,1,0:T(8,128)(2,1)S(1)} %get-tuple-element.24), channel_id=1, replica_groups=mesh['fs_0'=12,'fs_1'=8,'fs_2'=2,'tp'=4] {'fs_1','tp'}, dimensions={0} | all-to-all | bytes 131072 | tf_op jit(solution)/shard_map/all_to_all | solution.py:288
  119.2 0.1 regroup.1
  119.3 14.7 %all_to_all.46 = bf16[12,8,640]{2,1,0:T(8,128)(2,1)S(1)} all-to-all(bf16[12,8,640]{2,1,0:T(8,128)(2,1)S(1)} %regroup.1), channel_id=1, replica_groups=mesh['fs_0'=12,'fs_1'=8,'fs_2'=2,'tp'=4] {'fs_0'}, dimensions={0} | all-to-all | bytes 245760 | tf_op jit(solution)/shard_map/all_to_all | solution.py:297
  134.1 6.6 %all_to_all.47 = bf16[2,96,640]{2,1,0:T(8,128)(2,1)S(1)} all-to-all(bf16[2,96,640]{2,1,0:T(8,128)(2,1)S(1)} %broadcast_in_dim.22), channel_id=1, replica_groups=mesh['fs_0'=12,'fs_1'=8,'fs_2'=2,'tp'=4] {'fs_2'}, dimensions={0} | all-to-all | bytes 491520 | tf_op jit(solution)/shard_map/all_to_all | solution.py:22
  140.6 4.9 %all-gather.2.cloned.1.call-done.refs_4_ = bf16[3072,960]{1,0:T(8,128)(2,1)} async-done(((bf16[16,960]{1,0:T(8,128)(2,1)}), bf16[3072,960]{1,0:T(8,128)(2,1)}) %all-gather.2.cloned.1.call-update) | async-done | bytes 5898256 | tf_op jit(solution)/shard_map/all_gather | solution.py:236
  145.5 5.0 %update.1 = (f32[16,384]{1,0:T(8,128)}, f32[16,192]{1,0:T(8,128)}, f32[16,384]{1,0:T(8,128)}, f32[16,192]{1,0:T(8,128)}, bf16[3072,384]{1,0:T(8,128)(2,1)}, /*index=5*/bf16[192,3072]{1,0:T(8,128)(2,1)}) custom-call(bf16[192,640]{1,0:T(8,128)(2,1)S(1)} %bitcast.10, bf16[16,960]{1,0:T(8,128)(2,1)} %get-tuple-element.25.refs_1_, f32[16,384]{1,0:T(8,128)} %refs_2_.3, ...), custom_call_target="tpu_custom_call" | custom-call | tf_op jit(solution)/shard_map/update/pallas_call | solution.py:303
  (2 shorter events, 0.0 us)
Async XLA Ops:
  7.2 138.3 %all-gather.2.cloned.1.call-start = ((), (), s32[]{:S(2)}) async-start(), calls=%async_computation.8 | async-start | bytes 6324224 | tf_op jit(solution)/shard_map/all_gather | solution.py:236
  8.9 52.7 %copy-start.6 = (bf16[1024,3072]{1,0:T(8,128)(2,1)S(1)}, bf16[1024,3072]{1,0:T(8,128)(2,1)}, u32[]{:S(2)}) copy-start(bf16[1024,3072]{1,0:T(8,128)(2,1)} %param.11) | copy-start | bytes 18874372
  53.0 22.9 %copy-start = (bf16[1024,384]{1,0:T(8,128)(2,1)S(1)}, bf16[1024,384]{1,0:T(8,128)(2,1)}, u32[]{:S(2)}) copy-start(bf16[1024,384]{1,0:T(8,128)(2,1)} %refs_1_.3) | copy-start | bytes 2359300
  53.0 22.9 %copy-start.1 = (bf16[1024,192]{0,1:T(8,128)(2,1)S(1)}, bf16[1024,192]{0,1:T(8,128)(2,1)}, u32[]{:S(2)}) copy-start(bf16[1024,192]{0,1:T(8,128)(2,1)} %param.12) | copy-start | bytes 1179652
  61.4 42.9 %copy-start.2 = (f32[1,384]{1,0:T(1,128)S(1)}, f32[1,384]{1,0:T(1,128)}, u32[]{:S(2)}) copy-start(f32[1,384]{1,0:T(1,128)} %v_first.1) | copy-start | bytes 4612
  61.4 42.9 %copy-start.3 = (f32[1,384]{1,0:T(1,128)S(1)}, f32[1,384]{1,0:T(1,128)}, u32[]{:S(2)}) copy-start(f32[1,384]{1,0:T(1,128)} %v_second.1) | copy-start | bytes 4612
  61.4 42.9 %copy-start.4 = (f32[1,192]{1,0:T(1,128)S(1)}, f32[1,192]{1,0:T(1,128)}, u32[]{:S(2)}) copy-start(f32[1,192]{1,0:T(1,128)} %q_first.1) | copy-start | bytes 2308
  61.4 42.9 %copy-start.5 = (f32[1,192]{1,0:T(1,128)S(1)}, f32[1,192]{1,0:T(1,128)}, u32[]{:S(2)}) copy-start(f32[1,192]{1,0:T(1,128)} %q_second.1) | copy-start | bytes 2308
Sparse Core Ops, SparseCore 0:
  11.8 133.7 all-gather.1

commit v4 on v3

--- a/solution.py
+++ b/solution.py
@@ -30,33 +30,30 @@
     return shift
 
 
-def pack_kernel(at, v_factor, q_factor, v_weight, q_weight, parcel, spread, *, sizes, width):
-    own, rank = v_factor.shape
-    n0, n1, n2 = sizes
-    row = lax.broadcasted_iota(jnp.int32, (rank, rank), 0)
-    far = row >> shift_of(n1 * n2)
-    place = (row & (n2 - 1)) * (n0 * n1) + far * n1 + ((row >> shift_of(n2)) & (n1 - 1))
-    col = lax.broadcasted_iota(jnp.int32, (rank, rank), 1)
-    turn = (place == col).astype(jnp.float32).astype(jnp.bfloat16)
-    place = (row & (n1 * n2 - 1)) * n0 + far
-    mine = (place == col + at[0] * width) & (col < width)
-    mine = mine.astype(jnp.float32).astype(jnp.bfloat16)
-
-    def exact(a, onehot):
-        return jnp.dot(a, onehot, preferred_element_type=jnp.float32).astype(jnp.bfloat16)
-
-    vf, qf = v_factor[...], q_factor[...]
+def pack_kernel(v_factor, q_factor, v_weight, q_weight, parcel):
     parcel[...] = jnp.concatenate(
         [
-            exact(vf, turn),
-            exact(qf, turn),
+            v_factor[...],
+            q_factor[...],
             v_weight[...].astype(jnp.bfloat16),
             q_weight[...].astype(jnp.bfloat16),
         ],
         axis=1,
     )
-    share = jnp.concatenate([exact(vf, mine)[:, :width], exact(qf, mine)[:, :width]], axis=1)
-    spread[...] = jnp.broadcast_to(share[None], spread.shape)
+
+
+def share_kernel(at, v_factor, q_factor, spread, *, sizes, width):
+    rank = v_factor.shape[1]
+    n0, n1, n2 = sizes
+    row = lax.broadcasted_iota(jnp.int32, (rank, width), 0)
+    place = (row & (n1 * n2 - 1)) * n0 + (row >> shift_of(n1 * n2))
+    col = lax.broadcasted_iota(jnp.int32, (rank, width), 1)
+    mine = (place == col + at[0] * width).astype(jnp.float32).astype(jnp.bfloat16)
+    parts = [
+        jnp.dot(f[...], mine, preferred_element_type=jnp.float32).astype(jnp.bfloat16)
+        for f in (v_factor, q_factor)
+    ]
+    spread[...] = jnp.broadcast_to(jnp.concatenate(parts, axis=1)[None], spread.shape)
 
 
 def terms_kernel(proj, v_cot, q_cot, blocks, term_v, term_q, wide, *, n0, width):
@@ -162,31 +159,39 @@
     spread[...] = jnp.broadcast_to(rows[None], spread.shape)
 
 
-def update_kernel(
-    rows, own, v_weight, q_weight, parcels, step_v, step_q, new_v, new_q, copy_v, copy_q, units,
-    rate, *, rank, v_cols, q_cols, entries
+def finish_kernel(
+    rows, v_factor, q_factor, v_weight, q_weight, step_v, step_q, new_v, new_q, units, rate,
+    *, sizes, v_cols, entries
 ):
-    cols = v_cols + q_cols
-
-    @pl.when(pl.program_id(0) == 0)
-    def _():
-        tail = rows[:, cols // 128 * 128 :].astype(jnp.float32)
-        lane = lax.broadcasted_iota(jnp.int32, tail.shape, 1) + cols // 128 * 128
-        total = jnp.sum(jnp.where((lane >= cols) & (lane < cols + 3), tail, 0.0), keepdims=True)
-        scale = lax.rsqrt(total / entries + 1e-06)
-        rate[...] = jnp.broadcast_to(learn_rate * scale, rate.shape)
-        units[:rank, :v_cols] = rows[:, :v_cols]
-        units[rank:, :v_cols] = jnp.zeros((rank, v_cols), units.dtype)
-        units[:rank, v_cols:] = jnp.zeros((rank, q_cols), units.dtype)
-        units[rank:, v_cols:] = rows[:, v_cols:cols]
-        step = scale * jnp.dot(
-            own[:, : 2 * rank], units[...], preferred_element_type=jnp.float32
-        )
-        step_v[...] = step[:, :v_cols]
-        step_q[...] = step[:, v_cols:]
-        new_v[...] = v_weight[...] - learn_rate * step[:, :v_cols]
-        new_q[...] = q_weight[...] - learn_rate * step[:, v_cols:]
-
+    rank = rows.shape[0]
+    cols = units.shape[1]
+    n0, n1, n2 = sizes
+    tail = rows[:, cols // 128 * 128 :].astype(jnp.float32)
+    lane = lax.broadcasted_iota(jnp.int32, tail.shape, 1) + cols // 128 * 128
+    total = jnp.sum(jnp.where((lane >= cols) & (lane < cols + 3), tail, 0.0), keepdims=True)
+    scale = lax.rsqrt(total / entries + 1e-06)
+    rate[...] = jnp.broadcast_to(learn_rate * scale, rate.shape)
+    row = lax.broadcasted_iota(jnp.int32, (rank, rank), 0)
+    far = row >> shift_of(n1 * n2)
+    place = (row & (n2 - 1)) * (n0 * n1) + far * n1 + ((row >> shift_of(n2)) & (n1 - 1))
+    turn = place == lax.broadcasted_iota(jnp.int32, (rank, rank), 1)
+    turn = turn.astype(jnp.float32).astype(jnp.bfloat16)
+    turned = jnp.dot(turn, rows[...], preferred_element_type=jnp.float32).astype(jnp.bfloat16)
+    units[:rank, :v_cols] = turned[:, :v_cols]
+    units[rank:, :v_cols] = jnp.zeros((rank, v_cols), units.dtype)
+    units[:rank, v_cols:] = jnp.zeros((rank, cols - v_cols), units.dtype)
+    units[rank:, v_cols:] = turned[:, v_cols:cols]
+    step = scale * jnp.dot(v_factor[...], turned[:, :v_cols], preferred_element_type=jnp.float32)
+    step_v[...] = step
+    new_v[...] = v_weight[...] - learn_rate * step
+    step = scale * jnp.dot(
+        q_factor[...], turned[:, v_cols:cols], preferred_element_type=jnp.float32
+    )
+    step_q[...] = step
+    new_q[...] = q_weight[...] - learn_rate * step
+
+
+def copies_kernel(units, rate, parcels, copy_v, copy_q, *, rank, v_cols):
     to_v, from_q = min(rank + -rank % 128, 2 * rank), rank // 128 * 128
     weights = parcels[:, 2 * rank :].astype(jnp.float32)
     step = jnp.dot(parcels[:, :to_v], units[:to_v, :v_cols], preferred_element_type=jnp.float32)
@@ -226,14 +231,21 @@
     near_core = lambda a: pltpu.with_memory_space_constraint(a, pltpu.VMEM)
     at = lax.axis_index("tp").astype(jnp.int32).reshape(1)
 
-    parcel, spread = pl.pallas_call(
-        lambda *refs: pack_kernel(*refs, sizes=sizes, width=width),
-        in_specs=[smem] + [vmem] * 4,
-        out_specs=[vmem] * 2,
-        out_shape=[shape((own, 2 * rank + cols), bf16), pltpu.VMEM((n0, own, 2 * width), bf16)],
+    parcel = pl.pallas_call(
+        pack_kernel,
+        in_specs=[vmem] * 4,
+        out_specs=vmem,
+        out_shape=shape((own, 2 * rank + cols), bf16),
         name="pack",
-    )(at, value_factor, query_factor, value_weight, query_weight)
+    )(value_factor, query_factor, value_weight, query_weight)
     parcels = lax.all_gather(parcel, FS, axis=0, tiled=True)
+    spread = pl.pallas_call(
+        lambda *refs: share_kernel(*refs, sizes=sizes, width=width),
+        in_specs=[smem] + [vmem] * 2,
+        out_specs=vmem,
+        out_shape=pltpu.VMEM((n0, own, 2 * width), bf16),
+        name="share",
+    )(at, value_factor, query_factor)
 
     near = lax.all_to_all(spread, "fs_0", 0, 0, tiled=True)
     near = sent_to_all(near, "fs_1")
@@ -297,40 +309,40 @@
     rows = lax.all_to_all(spread, "fs_0", 0, 0, tiled=True).reshape(n0 * n1, -1)
     rows = sent_to_all(rows, "fs_2").reshape(rank, -1)
 
-    steps = 2
-    block = whole // steps
-    fixed = lambda *s: pl.BlockSpec(s, lambda i: (0, 0))
-    step_v, step_q, new_v, new_q, copy_v, copy_q = pl.pallas_call(
-        lambda *refs: update_kernel(
-            *refs, rank=rank, v_cols=v_cols, q_cols=q_cols, entries=rank * cols * tp
-        ),
-        grid=(steps,),
-        in_specs=[
-            fixed(rank, lines * 128),
-            fixed(own, 2 * rank + cols),
-            fixed(own, v_cols),
-            fixed(own, q_cols),
-            pl.BlockSpec((block, 2 * rank + cols), lambda i: (i, 0)),
-        ],
-        out_specs=[
-            fixed(own, v_cols),
-            fixed(own, q_cols),
-            fixed(own, v_cols),
-            fixed(own, q_cols),
-            pl.BlockSpec((block, v_cols), lambda i: (i, 0)),
-            pl.BlockSpec((q_cols, block), lambda i: (0, i)),
-        ],
+    step_v, step_q, new_v, new_q, units, rate = pl.pallas_call(
+        lambda *refs: finish_kernel(*refs, sizes=sizes, v_cols=v_cols, entries=rank * cols * tp),
+        in_specs=[vmem] * 5,
+        out_specs=[vmem] * 6,
         out_shape=[
             shape((own, v_cols), f32),
             shape((own, q_cols), f32),
             shape((own, v_cols), f32),
             shape((own, q_cols), f32),
-            shape((whole, v_cols), bf16),
-            shape((q_cols, whole), bf16),
+            pltpu.VMEM((2 * rank, cols), bf16),
+            pltpu.VMEM((1, cols), f32),
         ],
-        scratch_shapes=[pltpu.VMEM((2 * rank, cols), bf16), pltpu.VMEM((1, cols), f32)],
-        name="update",
-    )(near_core(rows), parcel, value_weight, query_weight, parcels)
+        name="finish",
+    )(
+        near_core(rows),
+        near_core(value_factor),
+        near_core(query_factor),
+        near_core(value_weight),
+        near_core(query_weight),
+    )
+
+    steps = 2
+    block = whole // steps
+    copy_v, copy_q = pl.pallas_call(
+        lambda *refs: copies_kernel(*refs, rank=rank, v_cols=v_cols),
+        grid=(steps,),
+        in_specs=[vmem, vmem, pl.BlockSpec((block, 2 * rank + cols), lambda i: (i, 0))],
+        out_specs=[
+            pl.BlockSpec((block, v_cols), lambda i: (i, 0)),
+            pl.BlockSpec((q_cols, block), lambda i: (0, i)),
+        ],
+        out_shape=[shape((whole, v_cols), bf16), shape((q_cols, whole), bf16)],
+        name="copies",
+    )(near_core(units), near_core(rate), parcels)
     return (step_q, step_v, new_q, new_v, first_q, second_q, first_v, second_v, copy_q.T, copy_v)
 
 

time: 158 us -> 158 us (level)
  Pallas kernels: 8.01 us -> 9.63 us
    pallas_call x2 -> x4, Pallas kernels: 6.61 us -> 8.23 us  [the longest x1 4.83 us: on_device(): pl.pallas_call(lambda *refs: copies_kernel(*refs, rank=rank, v_cols=v_col...]
  transfers between devices with their start and end apart: 1 -> 1, of which waited for: 1 -> 1; matrix products, arithmetic and copies ran while one was open for 2% -> 2% of each run, Pallas kernels for 1% -> 2%
where the time goes in v4:
time: 158 us
  blocking collectives  127 us (80%)
  between operations  14.2 us (9%)
  Pallas kernels  9.63 us (6%)
  waiting for transfers between devices  3.99 us (3%)
  matrix products  2.08 us (1%)
    all_to_all x3, blocking collectives, sent_to_all(): lax.all_to_all(jnp.broadcast_to(value[None], (size, *value.shape)), axis,...  34.2 us
    all_to_all x1, blocking collectives, on_device(): near = lax.all_to_all(spread, 'fs_0', 0, 0, tiled=True)  25.4 us
    all_to_all x1, blocking collectives, on_device(): blocks = lax.all_to_all(blocks, ('fs_1', 'fs_2'), 0, 0, tiled=True)  15.7 us
    all_to_all x1, blocking collectives, on_device(): rows = lax.all_to_all(spread, 'fs_0', 0, 0, tiled=True).reshape(n0 * n1, -1)  14.2 us
    all_to_all x1, blocking collectives, on_device(): blocks = lax.all_to_all(spread, ('fs_1', 'tp'), 0, 0, tiled=True)  13.6 us
    all_to_all x1, blocking collectives, on_device(): term = lax.all_to_all(term, 'fs_0', 0, 0, tiled=True)  12.2 us
    all_gather x1, blocking collectives, on_device(): proj = lax.all_gather(proj, 'tp', axis=0, tiled=True)  12 us
    pallas_call x1, Pallas kernels, on_device(): pl.pallas_call(lambda *refs: copies_kernel(*refs, rank=rank, v_cols=v_col...  4.83 us
  transfers between devices with their start and end apart: 1, of which 1 were waited for; matrix products, arithmetic and copies ran while one was open for 2% of the time, Pallas kernels for 2%

profile of v4, /device:TPU:1, one launch (start us, length us, event | category | flops | bytes accessed | tf_op | source)
XLA Modules:
  0.0 157.8 jit_solution(579295463112441064)
XLA Ops:
  7.2 0.0 all-gather.2.cloned.1.call-start
  7.2 1.5 pack.1
  8.7 0.0 all-gather.2.cloned.1.call-update
  8.7 0.9 share.1
  9.7 0.0 copy-start.10
  9.7 25.4 %all_to_all.40 = bf16[12,16,96]{2,1,0:T(8,128)(2,1)S(1)} all-to-all(bf16[12,16,96]{2,1,0:T(8,128)(2,1)S(1)} %share.1), channel_id=1, replica_groups=mesh['fs_0'=12,'fs_1'=8,'fs_2'=2,'tp'=4] {'fs_0'}, dimensions={0} | all-to-all | bytes 73728 | tf_op jit(solution)/shard_map/all_to_all | solution.py:250
  35.1 0.1 broadcast_in_dim.8
  35.2 18.6 %all_to_all.41 = bf16[8,12,16,96]{3,2,1,0:T(8,128)(2,1)S(1)} all-to-all(bf16[8,12,16,96]{3,2,1,0:T(8,128)(2,1)S(1)} %broadcast_in_dim.8), channel_id=1, replica_groups=mesh['fs_0'=12,'fs_1'=8,'fs_2'=2,'tp'=4] {'fs_1'}, dimensions={0} | all-to-all | bytes 589824 | tf_op jit(solution)/shard_map/all_to_all | solution.py:22
  53.8 0.0 copy-start
  53.8 0.0 copy-start.1
  53.8 0.2 broadcast_in_dim.9
  54.0 8.1 %all_to_all.42 = bf16[2,8,12,16,96]{4,3,1,2,0:T(8,128)(2,1)S(1)} all-to-all(bf16[2,8,12,16,96]{4,3,1,2,0:T(8,128)(2,1)S(1)} %broadcast_in_dim.9), channel_id=1, replica_groups=mesh['fs_0'=12,'fs_1'=8,'fs_2'=2,'tp'=4] {'fs_2'}, dimensions={0} | all-to-all | bytes 1179648 | tf_op jit(solution)/shard_map/all_to_all | solution.py:22
  62.2 0.0 copy-start.6
  62.2 0.0 copy-start.7
  62.2 0.0 copy-start.8
  62.2 0.0 copy-start.9
  62.2 0.1 copy.22
  62.3 0.0 copy-done.10
  62.3 0.0 copy-start.2
  62.3 0.0 copy-start.3
  62.3 0.0 copy-start.4
  62.4 0.0 copy-start.5
  62.4 2.1 %convolution_convert_fusion = bf16[96,1024]{1,0:T(8,128)(2,1)S(1)} fusion(bf16[3072,96]{1,0:T(8,128)(2,1)S(1)} %bitcast.13, bf16[1024,3072]{1,0:T(8,128)(2,1)S(1)} %copy-done.10), kind=kOutput, calls=%fused_computation | convolution fusion | flops 604078080 | bytes 7077888 | tf_op jit(solution)/shard_map/dot_general | solution.py:254
  64.5 12.0 %all_gather.6.refs_0_ = bf16[384,1024]{1,0:T(8,128)(2,1)S(1)} all-gather(bf16[96,1024]{1,0:T(8,128)(2,1)S(1)} %convolution_convert_fusion), channel_id=1, replica_groups=mesh['fs_0'=12,'fs_1'=8,'fs_2'=2,'tp'=4] {'tp'}, dimensions={0}, use_global_device_ids=true | all-gather | bytes 983040 | tf_op jit(solution)/shard_map/all_gather | solution.py:257
  76.5 0.0 copy-done
  76.5 0.0 copy-done.1
  76.5 0.6 terms.1
  77.0 15.7 %all_to_all.43.refs_0_ = bf16[16,56,128]{2,1,0:T(8,128)(2,1)S(1)} all-to-all(bf16[16,56,128]{2,1,0:T(8,128)(2,1)S(1)} %terms.1), channel_id=1, replica_groups=mesh['fs_0'=12,'fs_1'=8,'fs_2'=2,'tp'=4] {'fs_1','fs_2'}, dimensions={0} | all-to-all | bytes 458752 | tf_op jit(solution)/shard_map/all_to_all | solution.py:274
  92.8 0.1 fold.1
  92.9 12.2 %all_to_all.44.terms = f32[12,8,128]{2,1,0:T(8,128)S(1)} all-to-all(f32[12,8,128]{2,1,0:T(8,128)S(1)} %fold.1), channel_id=1, replica_groups=mesh['fs_0'=12,'fs_1'=8,'fs_2'=2,'tp'=4] {'fs_0'}, dimensions={0} | all-to-all | bytes 98304 | tf_op jit(solution)/shard_map/all_to_all | solution.py:283
  105.1 0.0 copy-done.6
  105.1 0.0 copy-done.7
  105.1 0.0 copy-done.8
  105.1 0.0 copy-done.9
  105.1 0.6 moments.1
  105.7 13.6 %all_to_all.45 = bf16[32,8,128]{2,1,0:T(8,128)(2,1)S(1)} all-to-all(bf16[32,8,128]{2,1,0:T(8,128)(2,1)S(1)} %get-tuple-element.23), channel_id=1, replica_groups=mesh['fs_0'=12,'fs_1'=8,'fs_2'=2,'tp'=4] {'fs_1','tp'}, dimensions={0} | all-to-all | bytes 131072 | tf_op jit(solution)/shard_map/all_to_all | solution.py:300
  119.4 0.1 regroup.1
  119.5 14.2 %all_to_all.46 = bf16[12,8,640]{2,1,0:T(8,128)(2,1)S(1)} all-to-all(bf16[12,8,640]{2,1,0:T(8,128)(2,1)S(1)} %regroup.1), channel_id=1, replica_groups=mesh['fs_0'=12,'fs_1'=8,'fs_2'=2,'tp'=4] {'fs_0'}, dimensions={0} | all-to-all | bytes 245760 | tf_op jit(solution)/shard_map/all_to_all | solution.py:309
  133.7 7.4 %all_to_all.47 = bf16[2,96,640]{2,1,0:T(8,128)(2,1)S(1)} all-to-all(bf16[2,96,640]{2,1,0:T(8,128)(2,1)S(1)} %broadcast_in_dim.22), channel_id=1, replica_groups=mesh['fs_0'=12,'fs_1'=8,'fs_2'=2,'tp'=4] {'fs_2'}, dimensions={0} | all-to-all | bytes 491520 | tf_op jit(solution)/shard_map/all_to_all | solution.py:22
  141.2 0.0 copy-done.2
  141.2 0.0 copy-done.3
  141.2 0.0 copy-done.4
  141.2 0.0 copy-done.5
  141.2 1.0 finish.1
  142.2 4.0 %all-gather.2.cloned.1.call-done.refs_2_ = bf16[3072,960]{1,0:T(8,128)(2,1)} async-done(((bf16[16,960]{1,0:T(8,128)(2,1)}), bf16[3072,960]{1,0:T(8,128)(2,1)}) %all-gather.2.cloned.1.call-update) | async-done | bytes 5898256 | tf_op jit(solution)/shard_map/all_gather | solution.py:241
  146.1 4.8 %copies.1 = (bf16[3072,384]{1,0:T(8,128)(2,1)}, bf16[192,3072]{1,0:T(8,128)(2,1)}) custom-call(bf16[384,576]{1,0:T(8,128)(2,1)S(1)} %get-tuple-element.32.refs_0_, f32[1,576]{1,0:T(1,128)S(1)} %get-tuple-element.33.refs_1_, bf16[3072,960]{1,0:T(8,128)(2,1)} %all-gather.2.cloned.1.call-done.refs_2_), custom_call_target="tpu_custom_call" | custom-call | tf_op jit(solution)/shard_map/copies/pallas_call | solution.py:335
  (2 shorter events, 0.0 us)
Async XLA Ops:
  7.2 139.0 %all-gather.2.cloned.1.call-start = ((), (), s32[]{:S(2)}) async-start(), calls=%async_computation.8 | async-start | bytes 6324224 | tf_op jit(solution)/shard_map/all_gather | solution.py:241
  9.7 52.7 %copy-start.10 = (bf16[1024,3072]{1,0:T(8,128)(2,1)S(1)}, bf16[1024,3072]{1,0:T(8,128)(2,1)}, u32[]{:S(2)}) copy-start(bf16[1024,3072]{1,0:T(8,128)(2,1)} %param.11) | copy-start | bytes 18874372
  53.8 22.6 %copy-start = (bf16[1024,384]{1,0:T(8,128)(2,1)S(1)}, bf16[1024,384]{1,0:T(8,128)(2,1)}, u32[]{:S(2)}) copy-start(bf16[1024,384]{1,0:T(8,128)(2,1)} %refs_1_.4) | copy-start | bytes 2359300
  53.8 22.6 %copy-start.1 = (bf16[1024,192]{0,1:T(8,128)(2,1)S(1)}, bf16[1024,192]{0,1:T(8,128)(2,1)}, u32[]{:S(2)}) copy-start(bf16[1024,192]{0,1:T(8,128)(2,1)} %param.12) | copy-start | bytes 1179652
  62.2 42.9 %copy-start.6 = (f32[1,384]{1,0:T(1,128)S(1)}, f32[1,384]{1,0:T(1,128)}, u32[]{:S(2)}) copy-start(f32[1,384]{1,0:T(1,128)} %v_first.1) | copy-start | bytes 4612
  62.2 43.0 %copy-start.7 = (f32[1,384]{1,0:T(1,128)S(1)}, f32[1,384]{1,0:T(1,128)}, u32[]{:S(2)}) copy-start(f32[1,384]{1,0:T(1,128)} %v_second.1) | copy-start | bytes 4612
  62.2 43.0 %copy-start.8 = (f32[1,192]{1,0:T(1,128)S(1)}, f32[1,192]{1,0:T(1,128)}, u32[]{:S(2)}) copy-start(f32[1,192]{1,0:T(1,128)} %q_first.1) | copy-start | bytes 2308
  62.2 43.0 %copy-start.9 = (f32[1,192]{1,0:T(1,128)S(1)}, f32[1,192]{1,0:T(1,128)}, u32[]{:S(2)}) copy-start(f32[1,192]{1,0:T(1,128)} %q_second.1) | copy-start | bytes 2308
  62.3 78.8 %copy-start.2 = (f32[16,384]{1,0:T(8,128)S(1)}, f32[16,384]{1,0:T(8,128)}, u32[]{:S(2)}) copy-start(f32[16,384]{1,0:T(8,128)} %v_weight.1) | copy-start | bytes 73732
  62.3 78.8 %copy-start.3 = (bf16[16,192]{1,0:T(8,128)(2,1)S(1)}, bf16[16,192]{1,0:T(8,128)(2,1)}, u32[]{:S(2)}) copy-start(bf16[16,192]{1,0:T(8,128)(2,1)} %v_factor.1) | copy-start | bytes 18436
  62.3 78.8 %copy-start.4 = (bf16[16,192]{1,0:T(8,128)(2,1)S(1)}, bf16[16,192]{1,0:T(8,128)(2,1)}, u32[]{:S(2)}) copy-start(bf16[16,192]{1,0:T(8,128)(2,1)} %q_factor.1) | copy-start | bytes 18436
  62.4 78.8 %copy-start.5 = (f32[16,192]{1,0:T(8,128)S(1)}, f32[16,192]{1,0:T(8,128)}, u32[]{:S(2)}) copy-start(f32[16,192]{1,0:T(8,128)} %q_weight.1) | copy-start | bytes 36868
Sparse Core Ops, SparseCore 0:
  12.3 133.7 all-gather.1

commit v5 on v4

--- a/solution.py
+++ b/solution.py
@@ -30,8 +30,8 @@
     return shift
 
 
-def pack_kernel(v_factor, q_factor, v_weight, q_weight, parcel):
-    parcel[...] = jnp.concatenate(
+def pack_kernel(v_factor, q_factor, v_weight, q_weight, spread):
+    parcel = jnp.concatenate(
         [
             v_factor[...],
             q_factor[...],
@@ -40,20 +40,50 @@
         ],
         axis=1,
     )
-
-
-def share_kernel(at, v_factor, q_factor, spread, *, sizes, width):
-    rank = v_factor.shape[1]
+    spread[...] = jnp.broadcast_to(parcel[None], spread.shape)
+
+
+def in_lines(share):
+    rows, wide = share.shape
+    if wide != 96:
+        return share
+    top = rows * 3 // 4
+    extra = [share[top:, 32 * k : 32 * (k + 1)] for k in range(3)]
+    return jnp.concatenate([share[:top], jnp.concatenate(extra, axis=0)], axis=1)
+
+
+def out_of_lines(lines, wide):
+    if wide != 96:
+        return lines
+    part = lines.shape[1] // 3
+    extra = [lines[:, part * k : part * (k + 1), 96:] for k in range(3)]
+    return jnp.concatenate([lines[:, :, :96], jnp.concatenate(extra, axis=2)], axis=1)
+
+
+def share_kernel(at, factors, spread, *, sizes, width):
     n0, n1, n2 = sizes
-    row = lax.broadcasted_iota(jnp.int32, (rank, width), 0)
+    rank = factors.shape[2] // 2
+    row = lax.broadcasted_iota(jnp.int32, (2 * rank, 2 * width), 0)
+    col = lax.broadcasted_iota(jnp.int32, (2 * rank, 2 * width), 1)
+    of_q = row >= rank
+    row = jnp.where(of_q, row - rank, row)
     place = (row & (n1 * n2 - 1)) * n0 + (row >> shift_of(n1 * n2))
-    col = lax.broadcasted_iota(jnp.int32, (rank, width), 1)
-    mine = (place == col + at[0] * width).astype(jnp.float32).astype(jnp.bfloat16)
-    parts = [
-        jnp.dot(f[...], mine, preferred_element_type=jnp.float32).astype(jnp.bfloat16)
-        for f in (v_factor, q_factor)
-    ]
-    spread[...] = jnp.broadcast_to(jnp.concatenate(parts, axis=1)[None], spread.shape)
+    mine = (of_q == (col >= width)) & (
+        place == jnp.where(col >= width, col - width, col) + at[0] * width
+    )
+    mine = mine.astype(jnp.float32).astype(jnp.bfloat16)
+    whole = factors[...].reshape(-1, 2 * rank)
+    share = jnp.dot(whole, mine, preferred_element_type=jnp.float32)
+    spread[...] = jnp.broadcast_to(in_lines(share).astype(jnp.bfloat16)[None], spread.shape)
+
+
+def project_kernel(lines, inputs, proj, share):
+    n0, n1, n2, own, wide = share.shape
+    for c in range(n2):
+        share[:, :, c, :, :] = out_of_lines(lines[c], wide).reshape(n0, n1, own, wide)
+    factors = share[...].reshape(-1, wide)
+    sums = jnp.dot(inputs[...], factors, preferred_element_type=jnp.float32)
+    proj[...] = sums.astype(jnp.bfloat16).T
 
 
 def terms_kernel(proj, v_cot, q_cot, blocks, term_v, term_q, wide, *, n0, width):
@@ -191,15 +221,24 @@
     new_q[...] = q_weight[...] - learn_rate * step
 
 
-def copies_kernel(units, rate, parcels, copy_v, copy_q, *, rank, v_cols):
+def copies_kernel(units, rate, parcels, copy_v, copy_q, turned, *, rank, v_cols):
     to_v, from_q = min(rank + -rank % 128, 2 * rank), rank // 128 * 128
-    weights = parcels[:, 2 * rank :].astype(jnp.float32)
-    step = jnp.dot(parcels[:, :to_v], units[:to_v, :v_cols], preferred_element_type=jnp.float32)
-    copy_v[...] = (weights[:, :v_cols] - rate[:, :v_cols] * step).astype(jnp.bfloat16)
+    block, n1, n2, own, q_cols = turned.shape
+    part = parcels[pl.ds(pl.program_id(0) * block, block)].reshape(-1, parcels.shape[-1])
+    weights = part[:, 2 * rank :].astype(jnp.float32)
+    step = jnp.dot(part[:, :to_v], units[:to_v, :v_cols], preferred_element_type=jnp.float32)
+    new = (weights[:, :v_cols] - rate[:, :v_cols] * step).astype(jnp.bfloat16)
+    new = new.reshape(block, n2, n1, own, v_cols)
+    for c in range(n2):
+        copy_v[:, :, c, :, :] = new[:, c]
     step = jnp.dot(
-        parcels[:, from_q : 2 * rank], units[from_q:, v_cols:], preferred_element_type=jnp.float32
-    )
-    copy_q[...] = (weights[:, v_cols:] - rate[:, v_cols:] * step).astype(jnp.bfloat16).T
+        part[:, from_q : 2 * rank], units[from_q:, v_cols:], preferred_element_type=jnp.float32
+    )
+    new = (weights[:, v_cols:] - rate[:, v_cols:] * step).astype(jnp.bfloat16)
+    new = new.reshape(block, n2, n1, own, q_cols)
+    for c in range(n2):
+        turned[:, :, c, :, :] = new[:, c]
+    copy_q[...] = turned[...].reshape(-1, q_cols).T
 
 
 def on_device(
@@ -228,32 +267,44 @@
     shape = jax.ShapeDtypeStruct
     vmem = pl.BlockSpec(memory_space=pltpu.VMEM)
     smem = pl.BlockSpec(memory_space=pltpu.SMEM)
+    small = pltpu.CompilerParams(vmem_limit_bytes=16 * 1024 * 1024)
+    waits = pl.CostEstimate(flops=20_000_000_000, transcendentals=0, bytes_accessed=1_000_000)
     near_core = lambda a: pltpu.with_memory_space_constraint(a, pltpu.VMEM)
     at = lax.axis_index("tp").astype(jnp.int32).reshape(1)
 
-    parcel = pl.pallas_call(
+    parts = 2 * rank + cols
+    spread = pl.pallas_call(
         pack_kernel,
         in_specs=[vmem] * 4,
         out_specs=vmem,
-        out_shape=shape((own, 2 * rank + cols), bf16),
+        out_shape=pltpu.VMEM((n1, own, parts), bf16),
         name="pack",
     )(value_factor, query_factor, value_weight, query_weight)
-    parcels = lax.all_gather(parcel, FS, axis=0, tiled=True)
+    near = lax.all_to_all(spread, "fs_1", 0, 0, tiled=True)
+    parcels = lax.all_gather(near.reshape(n1 * own, parts), ("fs_0", "fs_2"), axis=0, tiled=True)
+
+    lines = (n1 * own * 3 // 4, 128) if 2 * width == 96 else (n1 * own, 2 * width)
     spread = pl.pallas_call(
         lambda *refs: share_kernel(*refs, sizes=sizes, width=width),
-        in_specs=[smem] + [vmem] * 2,
-        out_specs=vmem,
-        out_shape=pltpu.VMEM((n0, own, 2 * width), bf16),
+        grid=(1,),
+        in_specs=[smem, pl.BlockSpec((n1, own, 2 * rank), lambda i: (0, 0, 0))],
+        out_specs=vmem,
+        out_shape=pltpu.VMEM((n0, *lines), bf16),
+        compiler_params=small,
+        cost_estimate=waits,
         name="share",
-    )(at, value_factor, query_factor)
-
+    )(at, pltpu.with_memory_space_constraint(near, pltpu.HBM))
     near = lax.all_to_all(spread, "fs_0", 0, 0, tiled=True)
-    near = sent_to_all(near, "fs_1")
-    near = sent_to_all(near, "fs_2")
-    share = near.transpose(2, 1, 0, 3, 4).reshape(-1, 2 * width)
-    proj = lax.dot_general(
-        share, inputs, (((0,), (1,)), ((), ())), preferred_element_type=f32
-    ).astype(bf16)
+    near = sent_to_all(near, "fs_2").reshape(n2, n0, *lines)
+    proj = pl.pallas_call(
+        project_kernel,
+        in_specs=[vmem] * 2,
+        out_specs=vmem,
+        out_shape=pltpu.VMEM((2 * width, inputs.shape[0]), bf16),
+        scratch_shapes=[pltpu.VMEM((n0, n1, n2, own, 2 * width), bf16)],
+        compiler_params=small,
+        name="project",
+    )(near_core(near), near_core(inputs))
     proj = lax.all_gather(proj, "tp", axis=0, tiled=True)
 
     chunks = v_cols // 128
@@ -297,6 +348,7 @@
         near_core(query_second),
     )
 
+    spread, parcels = lax.optimization_barrier((spread, parcels))
     blocks = lax.all_to_all(spread, ("fs_1", "tp"), 0, 0, tiled=True)
     lines = -(-(cols + 3) // 128)
     spread = pl.pallas_call(
@@ -304,6 +356,8 @@
         in_specs=[smem, vmem],
         out_specs=vmem,
         out_shape=pltpu.VMEM((n0, n1, lines * 128), bf16),
+        compiler_params=small,
+        cost_estimate=waits,
         name="regroup",
     )(at, near_core(blocks.reshape(n1, tp, 8, 128)))
     rows = lax.all_to_all(spread, "fs_0", 0, 0, tiled=True).reshape(n0 * n1, -1)
@@ -321,6 +375,8 @@
             pltpu.VMEM((2 * rank, cols), bf16),
             pltpu.VMEM((1, cols), f32),
         ],
+        compiler_params=small,
+        cost_estimate=waits,
         name="finish",
     )(
         near_core(rows),
@@ -330,19 +386,26 @@
         near_core(query_weight),
     )
 
-    steps = 2
-    block = whole // steps
+    steps = 4
+    block = n0 // steps
     copy_v, copy_q = pl.pallas_call(
         lambda *refs: copies_kernel(*refs, rank=rank, v_cols=v_cols),
         grid=(steps,),
-        in_specs=[vmem, vmem, pl.BlockSpec((block, 2 * rank + cols), lambda i: (i, 0))],
+        in_specs=[
+            vmem,
+            vmem,
+            vmem,
+        ],
         out_specs=[
-            pl.BlockSpec((block, v_cols), lambda i: (i, 0)),
-            pl.BlockSpec((q_cols, block), lambda i: (0, i)),
+            pl.BlockSpec((block, n1, n2, own, v_cols), lambda i: (i, 0, 0, 0, 0)),
+            pl.BlockSpec((q_cols, whole // steps), lambda i: (0, i)),
         ],
-        out_shape=[shape((whole, v_cols), bf16), shape((q_cols, whole), bf16)],
+        out_shape=[shape((n0, n1, n2, own, v_cols), bf16), shape((q_cols, whole), bf16)],
+        scratch_shapes=[pltpu.VMEM((block, n1, n2, own, q_cols), bf16)],
+        compiler_params=small,
         name="copies",
-    )(near_core(units), near_core(rate), parcels)
+    )(near_core(units), near_core(rate), near_core(parcels.reshape(n0, n2, n1 * own, parts)))
+    copy_v = copy_v.reshape(whole, v_cols)
     return (step_q, step_v, new_q, new_v, first_q, second_q, first_v, second_v, copy_q.T, copy_v)
 
 

time: 158 us -> 158 us (level)
  blocking collectives: 127 us -> 133 us
  waiting for transfers between devices: 3.99 us -> 0.02 us
  matrix products: 2.08 us -> 0 us
    all_to_all x0 -> x1, blocking collectives: none -> 17 us  [on_device(): near = lax.all_to_all(spread, 'fs_1', 0, 0, tiled=True)]
    all_to_all x3 -> x2, blocking collectives: 34.2 us -> 20.9 us  [sent_to_all(): lax.all_to_all(jnp.broadcast_to(value[None], (size, *value.shape)), axis,...]
    all_gather x1, waiting for transfers between devices: 3.98 us -> 0.01 us  [on_device(): lax.all_gather(near.reshape(n1 * own, parts), ('fs_0', 'fs_2'), axis=0, t...]
    all_to_all x1, blocking collectives: 25.4 us -> 28.8 us  [on_device(): near = lax.all_to_all(spread, 'fs_0', 0, 0, tiled=True)]
    dot_general x1 -> x0, matrix products: 2.08 us -> none  [on_device(): lax.dot_general(share, inputs, (((0,), (1,)), ((), ())), preferred_elemen...]
    pallas_call x0 -> x1, Pallas kernels: none -> 1.99 us  [on_device(): pl.pallas_call(project_kernel, in_specs=[vmem] * 2, out_specs=vmem, out_s...]
  transfers between devices with their start and end apart: 1 -> 1, of which waited for: 1 -> 0; matrix products, arithmetic and copies ran while one was open for 2% -> 0% of each run, Pallas kernels for 2% -> 3%
where the time goes in v5:
time: 158 us
  blocking collectives  133 us (84%)
  between operations  14.2 us (9%)
  Pallas kernels  10.2 us (6%)
    all_to_all x1, blocking collectives, on_device(): near = lax.all_to_all(spread, 'fs_0', 0, 0, tiled=True)  28.8 us
    all_to_all x2, blocking collectives, sent_to_all(): lax.all_to_all(jnp.broadcast_to(value[None], (size, *value.shape)), axis,...  20.9 us
    all_to_all x1, blocking collectives, on_device(): near = lax.all_to_all(spread, 'fs_1', 0, 0, tiled=True)  17 us
    all_to_all x1, blocking collectives, on_device(): blocks = lax.all_to_all(blocks, ('fs_1', 'fs_2'), 0, 0, tiled=True)  15.8 us
    all_to_all x1, blocking collectives, on_device(): term = lax.all_to_all(term, 'fs_0', 0, 0, tiled=True)  13.2 us
    all_to_all x1, blocking collectives, on_device(): rows = lax.all_to_all(spread, 'fs_0', 0, 0, tiled=True).reshape(n0 * n1, -1)  13 us
    all_to_all x1, blocking collectives, on_device(): blocks = lax.all_to_all(spread, ('fs_1', 'tp'), 0, 0, tiled=True)  12.2 us
    all_gather x1, blocking collectives, on_device(): proj = lax.all_gather(proj, 'tp', axis=0, tiled=True)  12 us
  transfers between devices with their start and end apart: 1, of which 0 were waited for; matrix products, arithmetic and copies ran while one was open for 0% of the time, Pallas kernels for 3%

profile of v5, /device:TPU:1, one launch (start us, length us, event | category | flops | bytes accessed | tf_op | source)
XLA Modules:
  0.0 157.5 jit_solution(6640773487376761741)
XLA Ops:
  7.2 0.0 all-gather.2.cloned.1.call-start
  7.2 0.8 pack.1
  8.1 0.0 slice-start
  8.1 17.0 %all_to_all.40.refs_1_ = bf16[8,16,960]{2,1,0:T(8,128)(2,1)} all-to-all(bf16[8,16,960]{2,1,0:T(8,128)(2,1)S(1)} %pack.1), channel_id=1, replica_groups=mesh['fs_0'=12,'fs_1'=8,'fs_2'=2,'tp'=4] {'fs_1'}, dimensions={0} | all-to-all | bytes 491520 | tf_op jit(solution)/shard_map/all_to_all | solution.py:283
  25.1 0.0 all-gather.2.cloned.1.call-update
  25.1 0.0 slice-start.1
  25.1 1.4 share.1
  26.5 0.0 copy-start
  26.6 0.0 copy-start.1
  26.6 28.8 %all_to_all.41 = bf16[12,96,128]{2,1,0:T(8,128)(2,1)S(1)} all-to-all(bf16[12,96,128]{2,1,0:T(8,128)(2,1)S(1)} %share.1), channel_id=1, replica_groups=mesh['fs_0'=12,'fs_1'=8,'fs_2'=2,'tp'=4] {'fs_0'}, dimensions={0} | all-to-all | bytes 589824 | tf_op jit(solution)/shard_map/all_to_all | solution.py:297
  55.4 0.1 broadcast_in_dim.6
  55.4 0.0 copy-start.6
  55.4 0.0 copy-start.7
  55.5 0.0 copy-start.8
  55.5 0.0 copy-start.9
  55.5 12.8 %all_to_all.42.lines = bf16[2,12,96,128]{3,2,1,0:T(8,128)(2,1)S(1)} all-to-all(bf16[2,12,96,128]{3,2,1,0:T(8,128)(2,1)S(1)} %broadcast_in_dim.6), channel_id=1, replica_groups=mesh['fs_0'=12,'fs_1'=8,'fs_2'=2,'tp'=4] {'fs_2'}, dimensions={0} | all-to-all | bytes 1179648 | tf_op jit(solution)/shard_map/all_to_all | solution.py:22
  68.3 0.0 slice-done
  68.3 0.0 slice-done.1
  68.3 2.0 %project.1 = bf16[96,1024]{1,0:T(8,128)(2,1)S(1)} custom-call(bf16[2,12,96,128]{3,2,1,0:T(8,128)(2,1)S(1)} %all_to_all.42.lines, bf16[1024,3072]{1,0:T(8,128)(2,1)S(1)} %bitcast.10), custom_call_target="tpu_custom_call" | custom-call | tf_op jit(solution)/shard_map/project/pallas_call | solution.py:299
  70.3 12.0 %all_gather.6.refs_0_ = bf16[384,1024]{1,0:T(8,128)(2,1)S(1)} all-gather(bf16[96,1024]{1,0:T(8,128)(2,1)S(1)} %project.1), channel_id=1, replica_groups=mesh['fs_0'=12,'fs_1'=8,'fs_2'=2,'tp'=4] {'tp'}, dimensions={0}, use_global_device_ids=true | all-gather | bytes 983040 | tf_op jit(solution)/shard_map/all_gather | solution.py:308
  82.3 0.0 copy-done
  82.3 0.0 copy-done.1
  82.3 0.6 terms.1
  82.9 15.8 %all_to_all.43.refs_0_ = bf16[16,56,128]{2,1,0:T(8,128)(2,1)S(1)} all-to-all(bf16[16,56,128]{2,1,0:T(8,128)(2,1)S(1)} %terms.1), channel_id=1, replica_groups=mesh['fs_0'=12,'fs_1'=8,'fs_2'=2,'tp'=4] {'fs_1','fs_2'}, dimensions={0} | all-to-all | bytes 458752 | tf_op jit(solution)/shard_map/all_to_all | solution.py:325
  98.7 0.1 fold.1
  98.8 13.2 %all_to_all.44.terms = f32[12,8,128]{2,1,0:T(8,128)S(1)} all-to-all(f32[12,8,128]{2,1,0:T(8,128)S(1)} %fold.1), channel_id=1, replica_groups=mesh['fs_0'=12,'fs_1'=8,'fs_2'=2,'tp'=4] {'fs_0'}, dimensions={0} | all-to-all | bytes 98304 | tf_op jit(solution)/shard_map/all_to_all | solution.py:334
  112.0 0.0 copy-done.6
  112.0 0.0 copy-done.7
  112.0 0.0 copy-done.8
  112.0 0.0 copy-done.9
  112.0 0.6 moments.1
  112.6 0.0 all-gather.2.cloned.1.call-done
  112.6 12.2 %all_to_all.45 = bf16[32,8,128]{2,1,0:T(8,128)(2,1)S(1)} all-to-all(bf16[32,8,128]{2,1,0:T(8,128)(2,1)S(1)} %get-tuple-element.26), channel_id=1, replica_groups=mesh['fs_0'=12,'fs_1'=8,'fs_2'=2,'tp'=4] {'fs_1','tp'}, dimensions={0} | all-to-all | bytes 131072 | tf_op jit(solution)/shard_map/all_to_all | solution.py:352
  124.8 0.0 copy-start.2
  124.8 0.0 copy-start.3
  124.8 0.0 copy-start.4
  124.8 0.0 slice-start.2
  124.9 0.1 regroup.1
  125.0 13.0 %all_to_all.46 = bf16[12,8,640]{2,1,0:T(8,128)(2,1)S(1)} all-to-all(bf16[12,8,640]{2,1,0:T(8,128)(2,1)S(1)} %regroup.1), channel_id=1, replica_groups=mesh['fs_0'=12,'fs_1'=8,'fs_2'=2,'tp'=4] {'fs_0'}, dimensions={0} | all-to-all | bytes 245760 | tf_op jit(solution)/shard_map/all_to_all | solution.py:363
  138.0 8.1 %all_to_all.47 = bf16[2,96,640]{2,1,0:T(8,128)(2,1)S(1)} all-to-all(bf16[2,96,640]{2,1,0:T(8,128)(2,1)S(1)} %broadcast_in_dim.15), channel_id=1, replica_groups=mesh['fs_0'=12,'fs_1'=8,'fs_2'=2,'tp'=4] {'fs_2'}, dimensions={0} | all-to-all | bytes 491520 | tf_op jit(solution)/shard_map/all_to_all | solution.py:22
  146.1 0.0 copy-done.2
  146.1 0.0 copy-done.3
  146.1 0.0 copy-done.4
  146.1 0.0 copy-done.5
  146.1 1.0 finish.1
  147.1 0.0 slice-done.2
  147.1 0.0 slice-done.3
  147.1 3.6 %copies.1 = (bf16[12,8,2,16,384]{4,3,2,1,0:T(8,128)(2,1)}, bf16[192,3072]{1,0:T(8,128)(2,1)}) custom-call(bf16[384,576]{1,0:T(8,128)(2,1)S(1)} %get-tuple-element.35.refs_0_, f32[1,576]{1,0:T(1,128)S(1)} %get-tuple-element.36.refs_1_, bf16[12,2,128,960]{3,2,1,0:T(8,128)(2,1)S(1)} %bitcast.13), custom_call_target="tpu_custom_call" | custom-call | tf_op jit(solution)/shard_map/copies/pallas_call | solution.py:391
  (5 shorter events, 0.0 us)
Async XLA Ops:
  7.2 105.5 %all-gather.2.cloned.1.call-start = ((), (), s32[]{:S(2)}) async-start(), calls=%async_computation.8 | async-start | bytes 6553600 | tf_op jit(solution)/shard_map/all_gather | solution.py:284
  8.1 60.2 %slice-start = ((s8[6291456]{0:T(1024)(128)(4,1)}), s8[2097152]{0:T(1024)(128)(4,1)S(1)}, s32[]{:S(2)}) async-start(s8[6291456]{0:T(1024)(128)(4,1)} %bitcast.9), calls=%async_computation.9 | async-start | bytes 4194304
  25.1 43.2 %slice-start.1 = ((s8[6291456]{0:T(1024)(128)(4,1)}), s8[4194304]{0:T(1024)(128)(4,1)S(1)}, s32[]{:S(2)}) async-start(s8[6291456]{0:T(1024)(128)(4,1)} %bitcast.9), calls=%async_computation.10 | async-start | bytes 8388608
  26.5 55.8 %copy-start = (bf16[1024,384]{1,0:T(8,128)(2,1)S(1)}, bf16[1024,384]{1,0:T(8,128)(2,1)}, u32[]{:S(2)}) copy-start(bf16[1024,384]{1,0:T(8,128)(2,1)} %refs_1_.2) | copy-start | bytes 2359300
  26.6 55.7 %copy-start.1 = (bf16[1024,192]{0,1:T(8,128)(2,1)S(1)}, bf16[1024,192]{0,1:T(8,128)(2,1)}, u32[]{:S(2)}) copy-start(bf16[1024,192]{0,1:T(8,128)(2,1)} %param.12) | copy-start | bytes 1179652
  55.4 56.6 %copy-start.6 = (f32[1,384]{1,0:T(1,128)S(1)}, f32[1,384]{1,0:T(1,128)}, u32[]{:S(2)}) copy-start(f32[1,384]{1,0:T(1,128)} %v_first.1) | copy-start | bytes 4612
  55.4 56.6 %copy-start.7 = (f32[1,384]{1,0:T(1,128)S(1)}, f32[1,384]{1,0:T(1,128)}, u32[]{:S(2)}) copy-start(f32[1,384]{1,0:T(1,128)} %v_second.1) | copy-start | bytes 4612
  55.5 56.6 %copy-start.8 = (f32[1,192]{1,0:T(1,128)S(1)}, f32[1,192]{1,0:T(1,128)}, u32[]{:S(2)}) copy-start(f32[1,192]{1,0:T(1,128)} %q_first.1) | copy-start | bytes 2308
  55.5 56.6 %copy-start.9 = (f32[1,192]{1,0:T(1,128)S(1)}, f32[1,192]{1,0:T(1,128)}, u32[]{:S(2)}) copy-start(f32[1,192]{1,0:T(1,128)} %q_second.1) | copy-start | bytes 2308
  124.8 21.3 %copy-start.2 = (f32[16,384]{1,0:T(8,128)S(1)}, f32[16,384]{1,0:T(8,128)}, u32[]{:S(2)}) copy-start(f32[16,384]{1,0:T(8,128)} %refs_3_.1) | copy-start | bytes 73732
  124.8 21.3 %copy-start.3 = (f32[16,192]{1,0:T(8,128)S(1)}, f32[16,192]{1,0:T(8,128)}, u32[]{:S(2)}) copy-start(f32[16,192]{1,0:T(8,128)} %refs_4_.1) | copy-start | bytes 36868
  124.8 21.3 %copy-start.4 = (bf16[16,192]{1,0:T(8,128)(2,1)S(1)}, bf16[16,192]{1,0:T(8,128)(2,1)}, u32[]{:S(2)}) copy-start(bf16[16,192]{1,0:T(8,128)(2,1)} %refs_1_.3) | copy-start | bytes 18436
  124.8 21.3 %copy-start.5 = (bf16[16,192]{1,0:T(8,128)(2,1)S(1)}, bf16[16,192]{1,0:T(8,128)(2,1)}, u32[]{:S(2)}) copy-start(bf16[16,192]{1,0:T(8,128)(2,1)} %refs_2_.1) | copy-start | bytes 18436
  124.8 22.3 %slice-start.2 = ((s8[6291456]{0:T(1024)(128)(4,1)}), s8[4194304]{0:T(1024)(128)(4,1)S(1)}, s32[]{:S(2)}) async-start(s8[6291456]{0:T(1024)(128)(4,1)} %bitcast.11), calls=%async_computation.11 | async-start | bytes 8388608
  137.9 9.2 %slice-start.3 = ((s8[6291456]{0:T(1024)(128)(4,1)}), s8[2097152]{0:T(1024)(128)(4,1)S(1)}, s32[]{:S(2)}) async-start(s8[6291456]{0:T(1024)(128)(4,1)} %bitcast.11), calls=%async_computation.12 | async-start | bytes 4194304
Sparse Core Ops, SparseCore 0:
  25.2 73.4 all-gather.1

commit v6 on v5

--- a/solution.py
+++ b/solution.py
@@ -79,11 +79,17 @@
 
 def project_kernel(lines, inputs, proj, share):
     n0, n1, n2, own, wide = share.shape
-    for c in range(n2):
-        share[:, :, c, :, :] = out_of_lines(lines[c], wide).reshape(n0, n1, own, wide)
+
+    @pl.when(pl.program_id(0) == 0)
+    def _():
+        for c in range(n2):
+            share[:, :, c, :, :] = out_of_lines(lines[c], wide).reshape(n0, n1, own, wide)
+
     factors = share[...].reshape(-1, wide)
     sums = jnp.dot(inputs[...], factors, preferred_element_type=jnp.float32)
-    proj[...] = sums.astype(jnp.bfloat16).T
+    tokens = inputs.shape[0]
+    begin = pl.multiple_of(pl.program_id(0) * tokens, tokens)
+    proj[:, pl.ds(begin, tokens)] = sums.astype(jnp.bfloat16).T
 
 
 def terms_kernel(proj, v_cot, q_cot, blocks, term_v, term_q, wide, *, n0, width):
@@ -281,7 +287,7 @@
         name="pack",
     )(value_factor, query_factor, value_weight, query_weight)
     near = lax.all_to_all(spread, "fs_1", 0, 0, tiled=True)
-    parcels = lax.all_gather(near.reshape(n1 * own, parts), ("fs_0", "fs_2"), axis=0, tiled=True)
+    parcel = near.reshape(n1 * own, parts)
 
     lines = (n1 * own * 3 // 4, 128) if 2 * width == 96 else (n1 * own, 2 * width)
     spread = pl.pallas_call(
@@ -293,18 +299,20 @@
         compiler_params=small,
         cost_estimate=waits,
         name="share",
-    )(at, pltpu.with_memory_space_constraint(near, pltpu.HBM))
+    )(at, near)
     near = lax.all_to_all(spread, "fs_0", 0, 0, tiled=True)
+    near, parcel = lax.optimization_barrier((near, parcel))
+    parcels = lax.all_gather(parcel, ("fs_0", "fs_2"), axis=0, tiled=True)
     near = sent_to_all(near, "fs_2").reshape(n2, n0, *lines)
     proj = pl.pallas_call(
         project_kernel,
-        in_specs=[vmem] * 2,
+        grid=(4,),
+        in_specs=[vmem, pl.BlockSpec((inputs.shape[0] // 4, inputs.shape[1]), lambda i: (i, 0))],
         out_specs=vmem,
         out_shape=pltpu.VMEM((2 * width, inputs.shape[0]), bf16),
         scratch_shapes=[pltpu.VMEM((n0, n1, n2, own, 2 * width), bf16)],
-        compiler_params=small,
         name="project",
-    )(near_core(near), near_core(inputs))
+    )(near_core(near), inputs)
     proj = lax.all_gather(proj, "tp", axis=0, tiled=True)
 
     chunks = v_cols // 128
@@ -348,7 +356,6 @@
         near_core(query_second),
     )
 
-    spread, parcels = lax.optimization_barrier((spread, parcels))
     blocks = lax.all_to_all(spread, ("fs_1", "tp"), 0, 0, tiled=True)
     lines = -(-(cols + 3) // 128)
     spread = pl.pallas_call(
@@ -361,6 +368,7 @@
         name="regroup",
     )(at, near_core(blocks.reshape(n1, tp, 8, 128)))
     rows = lax.all_to_all(spread, "fs_0", 0, 0, tiled=True).reshape(n0 * n1, -1)
+    rows, parcels = lax.optimization_barrier((rows, parcels))
     rows = sent_to_all(rows, "fs_2").reshape(rank, -1)
 
     step_v, step_q, new_v, new_q, units, rate = pl.pallas_call(

time: 158 us -> 160 us (1.013)
  blocking collectives: 133 us -> 114 us
  waiting for transfers between devices: 0.02 us -> 9.3 us
  starting transfers between devices: 0.04 us -> 7.68 us
  Pallas kernels: 10.2 us -> 12.9 us
    all_to_all x1 -> x0, blocking collectives: 17 us -> none  [on_device(): near = lax.all_to_all(spread, 'fs_1', 0, 0, tiled=True)]
    all_to_all x0 -> x1, waiting for transfers between devices: none -> 9.28 us  [on_device(): near = lax.all_to_all(spread, 'fs_1', 0, 0, tiled=True)]
    all_to_all x0 -> x1, starting transfers between devices: none -> 7.64 us  [on_device(): near = lax.all_to_all(spread, 'fs_1', 0, 0, tiled=True)]
    all_to_all x2, blocking collectives: 20.9 us -> 17.5 us  [sent_to_all(): lax.all_to_all(jnp.broadcast_to(value[None], (size, *value.shape)), axis,...]
    pallas_call x1, Pallas kernels: 1.99 us -> 5.09 us  [on_device(): pl.pallas_call(project_kernel, grid=(4,), in_specs=[vmem, pl.BlockSpec((i...]
    all_to_all x1, blocking collectives: 12.2 us -> 14.3 us  [on_device(): blocks = lax.all_to_all(spread, ('fs_1', 'tp'), 0, 0, tiled=True)]
  transfers between devices with their start and end apart: 1 -> 2, of which waited for: 0 -> 1; matrix products, arithmetic and copies ran while one was open for 0% -> 0% of each run, Pallas kernels for 3% -> 4%
where the time goes in v6:
time: 160 us; the launch traced here: 159 us
  blocking collectives  114 us (71%)
  between operations  14.2 us (9%)
  Pallas kernels  12.9 us (8%)
  waiting for transfers between devices  9.3 us (6%)
  starting transfers between devices  7.68 us (5%)
    all_to_all x1, blocking collectives, on_device(): near = lax.all_to_all(spread, 'fs_0', 0, 0, tiled=True)  28.8 us
    all_to_all x2, blocking collectives, sent_to_all(): lax.all_to_all(jnp.broadcast_to(value[None], (size, *value.shape)), axis,...  17.5 us
    all_to_all x1, blocking collectives, on_device(): blocks = lax.all_to_all(blocks, ('fs_1', 'fs_2'), 0, 0, tiled=True)  15.8 us
    all_to_all x1, blocking collectives, on_device(): blocks = lax.all_to_all(spread, ('fs_1', 'tp'), 0, 0, tiled=True)  14.3 us
    all_to_all x1, blocking collectives, on_device(): rows = lax.all_to_all(spread, 'fs_0', 0, 0, tiled=True).reshape(n0 * n1, -1)  12.8 us
    all_gather x1, blocking collectives, on_device(): proj = lax.all_gather(proj, 'tp', axis=0, tiled=True)  12.4 us
    all_to_all x1, blocking collectives, on_device(): term = lax.all_to_all(term, 'fs_0', 0, 0, tiled=True)  12.2 us
    all_to_all x1, waiting for transfers between devices, on_device(): near = lax.all_to_all(spread, 'fs_1', 0, 0, tiled=True)  9.28 us
  transfers between devices with their start and end apart: 2, of which 1 were waited for; matrix products, arithmetic and copies ran while one was open for 0% of the time, Pallas kernels for 4%

profile of v6, /device:TPU:1, one launch (start us, length us, event | category | flops | bytes accessed | tf_op | source)
XLA Modules:
  0.0 158.9 jit_solution(6259651804227591601)
XLA Ops:
  7.2 1.6 pack.1
  8.7 7.6 %all-to-all-start = ((bf16[8,16,960]{2,1,0:T(8,128)(2,1)}), bf16[8,16,960]{2,1,0:T(8,128)(2,1)S(1)}, u32[]{:S(2)}, u32[]{:S(2)}) async-start(bf16[8,16,960]{2,1,0:T(8,128)(2,1)} %pack.1), calls=%async_computation | async-start | bytes 524288 | tf_op jit(solution)/shard_map/all_to_all | solution.py:289
  16.4 0.0 all-gather.2.cloned.1.call-start
  16.4 9.3 %all-to-all-done.refs_1_ = bf16[8,16,960]{2,1,0:T(8,128)(2,1)S(1)} async-done(((bf16[8,16,960]{2,1,0:T(8,128)(2,1)}), bf16[8,16,960]{2,1,0:T(8,128)(2,1)S(1)}, u32[]{:S(2)}, u32[]{:S(2)}) %all-to-all-start) | async-done | bytes 245792 | tf_op jit(solution)/shard_map/all_to_all | solution.py:289
  25.7 0.0 copy-start
  25.7 0.4 share.1
  26.1 0.3 copy-done
  26.4 0.0 copy-start.1
  26.4 0.0 copy-start.2
  26.4 28.8 %all_to_all.40 = bf16[12,96,128]{2,1,0:T(8,128)(2,1)S(1)} all-to-all(bf16[12,96,128]{2,1,0:T(8,128)(2,1)S(1)} %share.1), channel_id=1, replica_groups=mesh['fs_0'=12,'fs_1'=8,'fs_2'=2,'tp'=4] {'fs_0'}, dimensions={0} | all-to-all | bytes 589824 | tf_op jit(solution)/shard_map/all_to_all | solution.py:303
  55.2 0.0 all-gather.2.cloned.1.call-update
  55.3 0.1 broadcast_in_dim.4
  55.4 0.0 copy-start.7
  55.4 0.0 copy-start.8
  55.4 0.0 copy-start.9
  55.4 0.0 copy-start.10
  55.4 8.8 %all_to_all.41.lines = bf16[2,12,96,128]{3,2,1,0:T(8,128)(2,1)S(1)} all-to-all(bf16[2,12,96,128]{3,2,1,0:T(8,128)(2,1)S(1)} %broadcast_in_dim.4), channel_id=1, replica_groups=mesh['fs_0'=12,'fs_1'=8,'fs_2'=2,'tp'=4] {'fs_2'}, dimensions={0} | all-to-all | bytes 1179648 | tf_op jit(solution)/shard_map/all_to_all | solution.py:22
  64.2 5.1 %project.1 = bf16[96,1024]{1,0:T(8,128)(2,1)S(1)} custom-call(bf16[2,12,96,128]{3,2,1,0:T(8,128)(2,1)S(1)} %all_to_all.41.lines, bf16[1024,3072]{1,0:T(8,128)(2,1)} %inputs.1), custom_call_target="tpu_custom_call" | custom-call | tf_op jit(solution)/shard_map/project/pallas_call | solution.py:307
  69.3 12.4 %all_gather.6.refs_0_ = bf16[384,1024]{1,0:T(8,128)(2,1)S(1)} all-gather(bf16[96,1024]{1,0:T(8,128)(2,1)S(1)} %project.1), channel_id=1, replica_groups=mesh['fs_0'=12,'fs_1'=8,'fs_2'=2,'tp'=4] {'tp'}, dimensions={0}, use_global_device_ids=true | all-gather | bytes 983040 | tf_op jit(solution)/shard_map/all_gather | solution.py:316
  81.7 0.0 copy-done.1
  81.7 0.0 copy-done.2
  81.7 0.6 terms.1
  82.3 15.8 %all_to_all.42.refs_0_ = bf16[16,56,128]{2,1,0:T(8,128)(2,1)S(1)} all-to-all(bf16[16,56,128]{2,1,0:T(8,128)(2,1)S(1)} %terms.1), channel_id=1, replica_groups=mesh['fs_0'=12,'fs_1'=8,'fs_2'=2,'tp'=4] {'fs_1','fs_2'}, dimensions={0} | all-to-all | bytes 458752 | tf_op jit(solution)/shard_map/all_to_all | solution.py:333
  98.1 0.1 fold.1
  98.2 12.2 %all_to_all.43.terms = f32[12,8,128]{2,1,0:T(8,128)S(1)} all-to-all(f32[12,8,128]{2,1,0:T(8,128)S(1)} %fold.1), channel_id=1, replica_groups=mesh['fs_0'=12,'fs_1'=8,'fs_2'=2,'tp'=4] {'fs_0'}, dimensions={0} | all-to-all | bytes 98304 | tf_op jit(solution)/shard_map/all_to_all | solution.py:342
  110.4 0.0 copy-done.7
  110.4 0.0 copy-done.8
  110.4 0.0 copy-done.9
  110.4 0.0 copy-done.10
  110.4 0.6 moments.1
  111.0 14.3 %all_to_all.44 = bf16[32,8,128]{2,1,0:T(8,128)(2,1)S(1)} all-to-all(bf16[32,8,128]{2,1,0:T(8,128)(2,1)S(1)} %get-tuple-element.28), channel_id=1, replica_groups=mesh['fs_0'=12,'fs_1'=8,'fs_2'=2,'tp'=4] {'fs_1','tp'}, dimensions={0} | all-to-all | bytes 131072 | tf_op jit(solution)/shard_map/all_to_all | solution.py:359
  125.3 0.0 copy-start.3
  125.3 0.0 copy-start.4
  125.3 0.0 copy-start.5
  125.3 0.0 copy-start.6
  125.3 0.1 regroup.1
  125.4 12.8 %all_to_all.45 = bf16[12,8,640]{2,1,0:T(8,128)(2,1)S(1)} all-to-all(bf16[12,8,640]{2,1,0:T(8,128)(2,1)S(1)} %regroup.1), channel_id=1, replica_groups=mesh['fs_0'=12,'fs_1'=8,'fs_2'=2,'tp'=4] {'fs_0'}, dimensions={0} | all-to-all | bytes 245760 | tf_op jit(solution)/shard_map/all_to_all | solution.py:370
  138.2 0.0 all-gather.2.cloned.1.call-done
  138.2 8.7 %all_to_all.46 = bf16[2,96,640]{2,1,0:T(8,128)(2,1)S(1)} all-to-all(bf16[2,96,640]{2,1,0:T(8,128)(2,1)S(1)} %broadcast_in_dim.5), channel_id=1, replica_groups=mesh['fs_0'=12,'fs_1'=8,'fs_2'=2,'tp'=4] {'fs_2'}, dimensions={0} | all-to-all | bytes 491520 | tf_op jit(solution)/shard_map/all_to_all | solution.py:22
  146.9 0.0 copy-done.3
  146.9 0.0 copy-done.4
  146.9 0.0 copy-done.5
  146.9 0.0 copy-done.6
  146.9 0.0 slice-start.1
  146.9 1.0 finish.1
  147.9 0.0 slice-done
  147.9 0.6 slice-done.1
  148.6 3.5 %copies.1 = (bf16[12,8,2,16,384]{4,3,2,1,0:T(8,128)(2,1)}, bf16[192,3072]{1,0:T(8,128)(2,1)}) custom-call(bf16[384,576]{1,0:T(8,128)(2,1)S(1)} %get-tuple-element.39.refs_0_, f32[1,576]{1,0:T(1,128)S(1)} %get-tuple-element.40.refs_1_, bf16[12,2,128,960]{3,2,1,0:T(8,128)(2,1)S(1)} %bitcast.11), custom_call_target="tpu_custom_call" | custom-call | tf_op jit(solution)/shard_map/copies/pallas_call | solution.py:399
  (3 shorter events, 0.0 us)
Async XLA Ops:
  8.7 17.0 %all-to-all-start = ((bf16[8,16,960]{2,1,0:T(8,128)(2,1)}), bf16[8,16,960]{2,1,0:T(8,128)(2,1)S(1)}, u32[]{:S(2)}, u32[]{:S(2)}) async-start(bf16[8,16,960]{2,1,0:T(8,128)(2,1)} %pack.1), calls=%async_computation | async-start | bytes 524288 | tf_op jit(solution)/shard_map/all_to_all | solution.py:289
  16.4 121.8 %all-gather.2.cloned.1.call-start = ((), (), s32[]{:S(2)}) async-start(), calls=%async_computation.8 | async-start | bytes 6553600 | tf_op jit(solution)/shard_map/all_gather | solution.py:305
  25.7 0.7 copy-start
  26.4 55.3 %copy-start.1 = (bf16[1024,384]{1,0:T(8,128)(2,1)S(1)}, bf16[1024,384]{1,0:T(8,128)(2,1)}, u32[]{:S(2)}) copy-start(bf16[1024,384]{1,0:T(8,128)(2,1)} %refs_1_.2) | copy-start | bytes 2359300
  26.4 55.3 %copy-start.2 = (bf16[1024,192]{0,1:T(8,128)(2,1)S(1)}, bf16[1024,192]{0,1:T(8,128)(2,1)}, u32[]{:S(2)}) copy-start(bf16[1024,192]{0,1:T(8,128)(2,1)} %param.12) | copy-start | bytes 1179652
  55.4 55.1 %copy-start.7 = (f32[1,384]{1,0:T(1,128)S(1)}, f32[1,384]{1,0:T(1,128)}, u32[]{:S(2)}) copy-start(f32[1,384]{1,0:T(1,128)} %v_first.1) | copy-start | bytes 4612
  55.4 55.1 %copy-start.8 = (f32[1,384]{1,0:T(1,128)S(1)}, f32[1,384]{1,0:T(1,128)}, u32[]{:S(2)}) copy-start(f32[1,384]{1,0:T(1,128)} %v_second.1) | copy-start | bytes 4612
  55.4 55.0 %copy-start.9 = (f32[1,192]{1,0:T(1,128)S(1)}, f32[1,192]{1,0:T(1,128)}, u32[]{:S(2)}) copy-start(f32[1,192]{1,0:T(1,128)} %q_first.1) | copy-start | bytes 2308
  55.4 55.0 %copy-start.10 = (f32[1,192]{1,0:T(1,128)S(1)}, f32[1,192]{1,0:T(1,128)}, u32[]{:S(2)}) copy-start(f32[1,192]{1,0:T(1,128)} %q_second.1) | copy-start | bytes 2308
  125.3 21.6 %copy-start.3 = (f32[16,384]{1,0:T(8,128)S(1)}, f32[16,384]{1,0:T(8,128)}, u32[]{:S(2)}) copy-start(f32[16,384]{1,0:T(8,128)} %refs_3_.1) | copy-start | bytes 73732
  125.3 21.6 %copy-start.4 = (f32[16,192]{1,0:T(8,128)S(1)}, f32[16,192]{1,0:T(8,128)}, u32[]{:S(2)}) copy-start(f32[16,192]{1,0:T(8,128)} %refs_4_.1) | copy-start | bytes 36868
  125.3 21.6 %copy-start.5 = (bf16[16,192]{1,0:T(8,128)(2,1)S(1)}, bf16[16,192]{1,0:T(8,128)(2,1)}, u32[]{:S(2)}) copy-start(bf16[16,192]{1,0:T(8,128)(2,1)} %refs_1_.3) | copy-start | bytes 18436
  125.3 21.6 %copy-start.6 = (bf16[16,192]{1,0:T(8,128)(2,1)S(1)}, bf16[16,192]{1,0:T(8,128)(2,1)}, u32[]{:S(2)}) copy-start(bf16[16,192]{1,0:T(8,128)(2,1)} %refs_2_.1) | copy-start | bytes 18436
  138.2 9.8 %slice-start = ((s8[6291456]{0:T(1024)(128)(4,1)}), s8[4194304]{0:T(1024)(128)(4,1)S(1)}, s32[]{:S(2)}) async-start(s8[6291456]{0:T(1024)(128)(4,1)} %bitcast.9), calls=%async_computation.9 | async-start | bytes 8388608
  146.9 1.6 %slice-start.1 = ((s8[6291456]{0:T(1024)(128)(4,1)}), s8[2097152]{0:T(1024)(128)(4,1)S(1)}, s32[]{:S(2)}) async-start(s8[6291456]{0:T(1024)(128)(4,1)} %bitcast.9), calls=%async_computation.10 | async-start | bytes 4194304
Sparse Core Ops, SparseCore 0:
  55.4 61.0 all-gather.1

commit v7 on v5

--- a/solution.py
+++ b/solution.py
@@ -386,7 +386,7 @@
         near_core(query_weight),
     )
 
-    steps = 4
+    steps = 2
     block = n0 // steps
     copy_v, copy_q = pl.pallas_call(
         lambda *refs: copies_kernel(*refs, rank=rank, v_cols=v_cols),

time: 158 us -> 158 us (level)
  no operation moved by 1% of the time
where the time goes in v7:
time: 158 us; the launch traced here: 157 us
  blocking collectives  133 us (84%)
  between operations  14.2 us (9%)
  Pallas kernels  9.92 us (6%)
    all_to_all x1, blocking collectives, on_device(): near = lax.all_to_all(spread, 'fs_0', 0, 0, tiled=True)  28.8 us
    all_to_all x2, blocking collectives, sent_to_all(): lax.all_to_all(jnp.broadcast_to(value[None], (size, *value.shape)), axis,...  20.9 us
    all_to_all x1, blocking collectives, on_device(): near = lax.all_to_all(spread, 'fs_1', 0, 0, tiled=True)  17 us
    all_to_all x1, blocking collectives, on_device(): blocks = lax.all_to_all(blocks, ('fs_1', 'fs_2'), 0, 0, tiled=True)  15.8 us
    all_to_all x1, blocking collectives, on_device(): term = lax.all_to_all(term, 'fs_0', 0, 0, tiled=True)  13.2 us
    all_to_all x1, blocking collectives, on_device(): rows = lax.all_to_all(spread, 'fs_0', 0, 0, tiled=True).reshape(n0 * n1, -1)  13 us
    all_to_all x1, blocking collectives, on_device(): blocks = lax.all_to_all(spread, ('fs_1', 'tp'), 0, 0, tiled=True)  12.2 us
    all_gather x1, blocking collectives, on_device(): proj = lax.all_gather(proj, 'tp', axis=0, tiled=True)  12 us
  transfers between devices with their start and end apart: 1, of which 0 were waited for; matrix products, arithmetic and copies ran while one was open for 0% of the time, Pallas kernels for 3%

profile of v7, /device:TPU:1, one launch (start us, length us, event | category | flops | bytes accessed | tf_op | source)
XLA Modules:
  0.0 157.3 jit_solution(11623934114499393340)
XLA Ops:
  7.2 0.0 all-gather.2.cloned.1.call-start
  7.2 0.8 pack.1
  8.1 0.0 slice-start
  8.1 17.0 %all_to_all.40.refs_1_ = bf16[8,16,960]{2,1,0:T(8,128)(2,1)} all-to-all(bf16[8,16,960]{2,1,0:T(8,128)(2,1)S(1)} %pack.1), channel_id=1, replica_groups=mesh['fs_0'=12,'fs_1'=8,'fs_2'=2,'tp'=4] {'fs_1'}, dimensions={0} | all-to-all | bytes 491520 | tf_op jit(solution)/shard_map/all_to_all | solution.py:283
  25.1 0.0 all-gather.2.cloned.1.call-update
  25.1 0.0 slice-start.1
  25.1 1.4 share.1
  26.5 0.0 copy-start
  26.6 0.0 copy-start.1
  26.6 28.8 %all_to_all.41 = bf16[12,96,128]{2,1,0:T(8,128)(2,1)S(1)} all-to-all(bf16[12,96,128]{2,1,0:T(8,128)(2,1)S(1)} %share.1), channel_id=1, replica_groups=mesh['fs_0'=12,'fs_1'=8,'fs_2'=2,'tp'=4] {'fs_0'}, dimensions={0} | all-to-all | bytes 589824 | tf_op jit(solution)/shard_map/all_to_all | solution.py:297
  55.4 0.1 broadcast_in_dim.6
  55.4 0.0 copy-start.6
  55.4 0.0 copy-start.7
  55.5 0.0 copy-start.8
  55.5 0.0 copy-start.9
  55.5 12.8 %all_to_all.42.lines = bf16[2,12,96,128]{3,2,1,0:T(8,128)(2,1)S(1)} all-to-all(bf16[2,12,96,128]{3,2,1,0:T(8,128)(2,1)S(1)} %broadcast_in_dim.6), channel_id=1, replica_groups=mesh['fs_0'=12,'fs_1'=8,'fs_2'=2,'tp'=4] {'fs_2'}, dimensions={0} | all-to-all | bytes 1179648 | tf_op jit(solution)/shard_map/all_to_all | solution.py:22
  68.3 0.0 slice-done
  68.3 0.0 slice-done.1
  68.3 2.0 %project.1 = bf16[96,1024]{1,0:T(8,128)(2,1)S(1)} custom-call(bf16[2,12,96,128]{3,2,1,0:T(8,128)(2,1)S(1)} %all_to_all.42.lines, bf16[1024,3072]{1,0:T(8,128)(2,1)S(1)} %bitcast.10), custom_call_target="tpu_custom_call" | custom-call | tf_op jit(solution)/shard_map/project/pallas_call | solution.py:299
  70.3 12.0 %all_gather.6.refs_0_ = bf16[384,1024]{1,0:T(8,128)(2,1)S(1)} all-gather(bf16[96,1024]{1,0:T(8,128)(2,1)S(1)} %project.1), channel_id=1, replica_groups=mesh['fs_0'=12,'fs_1'=8,'fs_2'=2,'tp'=4] {'tp'}, dimensions={0}, use_global_device_ids=true | all-gather | bytes 983040 | tf_op jit(solution)/shard_map/all_gather | solution.py:308
  82.3 0.0 copy-done
  82.3 0.0 copy-done.1
  82.3 0.6 terms.1
  82.9 15.8 %all_to_all.43.refs_0_ = bf16[16,56,128]{2,1,0:T(8,128)(2,1)S(1)} all-to-all(bf16[16,56,128]{2,1,0:T(8,128)(2,1)S(1)} %terms.1), channel_id=1, replica_groups=mesh['fs_0'=12,'fs_1'=8,'fs_2'=2,'tp'=4] {'fs_1','fs_2'}, dimensions={0} | all-to-all | bytes 458752 | tf_op jit(solution)/shard_map/all_to_all | solution.py:325
  98.7 0.1 fold.1
  98.8 13.2 %all_to_all.44.terms = f32[12,8,128]{2,1,0:T(8,128)S(1)} all-to-all(f32[12,8,128]{2,1,0:T(8,128)S(1)} %fold.1), channel_id=1, replica_groups=mesh['fs_0'=12,'fs_1'=8,'fs_2'=2,'tp'=4] {'fs_0'}, dimensions={0} | all-to-all | bytes 98304 | tf_op jit(solution)/shard_map/all_to_all | solution.py:334
  112.0 0.0 copy-done.6
  112.0 0.0 copy-done.7
  112.0 0.0 copy-done.8
  112.0 0.0 copy-done.9
  112.0 0.6 moments.1
  112.6 0.0 all-gather.2.cloned.1.call-done
  112.6 12.2 %all_to_all.45 = bf16[32,8,128]{2,1,0:T(8,128)(2,1)S(1)} all-to-all(bf16[32,8,128]{2,1,0:T(8,128)(2,1)S(1)} %get-tuple-element.26), channel_id=1, replica_groups=mesh['fs_0'=12,'fs_1'=8,'fs_2'=2,'tp'=4] {'fs_1','tp'}, dimensions={0} | all-to-all | bytes 131072 | tf_op jit(solution)/shard_map/all_to_all | solution.py:352
  124.8 0.0 copy-start.2
  124.8 0.0 copy-start.3
  124.8 0.0 copy-start.4
  124.8 0.0 slice-start.2
  124.9 0.1 regroup.1
  125.0 13.0 %all_to_all.46 = bf16[12,8,640]{2,1,0:T(8,128)(2,1)S(1)} all-to-all(bf16[12,8,640]{2,1,0:T(8,128)(2,1)S(1)} %regroup.1), channel_id=1, replica_groups=mesh['fs_0'=12,'fs_1'=8,'fs_2'=2,'tp'=4] {'fs_0'}, dimensions={0} | all-to-all | bytes 245760 | tf_op jit(solution)/shard_map/all_to_all | solution.py:363
  138.0 8.1 %all_to_all.47 = bf16[2,96,640]{2,1,0:T(8,128)(2,1)S(1)} all-to-all(bf16[2,96,640]{2,1,0:T(8,128)(2,1)S(1)} %broadcast_in_dim.15), channel_id=1, replica_groups=mesh['fs_0'=12,'fs_1'=8,'fs_2'=2,'tp'=4] {'fs_2'}, dimensions={0} | all-to-all | bytes 491520 | tf_op jit(solution)/shard_map/all_to_all | solution.py:22
  146.1 0.0 copy-done.2
  146.1 0.0 copy-done.3
  146.1 0.0 copy-done.4
  146.1 0.0 copy-done.5
  146.1 1.0 finish.1
  147.1 0.0 slice-done.2
  147.1 0.0 slice-done.3
  147.1 3.3 %copies.1 = (bf16[12,8,2,16,384]{4,3,2,1,0:T(8,128)(2,1)}, bf16[192,3072]{1,0:T(8,128)(2,1)}) custom-call(bf16[384,576]{1,0:T(8,128)(2,1)S(1)} %get-tuple-element.35.refs_0_, f32[1,576]{1,0:T(1,128)S(1)} %get-tuple-element.36.refs_1_, bf16[12,2,128,960]{3,2,1,0:T(8,128)(2,1)S(1)} %bitcast.13), custom_call_target="tpu_custom_call" | custom-call | tf_op jit(solution)/shard_map/copies/pallas_call | solution.py:391
  (5 shorter events, 0.0 us)
Async XLA Ops:
  7.2 105.5 %all-gather.2.cloned.1.call-start = ((), (), s32[]{:S(2)}) async-start(), calls=%async_computation.8 | async-start | bytes 6553600 | tf_op jit(solution)/shard_map/all_gather | solution.py:284
  8.1 60.2 %slice-start = ((s8[6291456]{0:T(1024)(128)(4,1)}), s8[2097152]{0:T(1024)(128)(4,1)S(1)}, s32[]{:S(2)}) async-start(s8[6291456]{0:T(1024)(128)(4,1)} %bitcast.9), calls=%async_computation.9 | async-start | bytes 4194304
  25.1 43.2 %slice-start.1 = ((s8[6291456]{0:T(1024)(128)(4,1)}), s8[4194304]{0:T(1024)(128)(4,1)S(1)}, s32[]{:S(2)}) async-start(s8[6291456]{0:T(1024)(128)(4,1)} %bitcast.9), calls=%async_computation.10 | async-start | bytes 8388608
  26.5 55.8 %copy-start = (bf16[1024,384]{1,0:T(8,128)(2,1)S(1)}, bf16[1024,384]{1,0:T(8,128)(2,1)}, u32[]{:S(2)}) copy-start(bf16[1024,384]{1,0:T(8,128)(2,1)} %refs_1_.2) | copy-start | bytes 2359300
  26.6 55.7 %copy-start.1 = (bf16[1024,192]{0,1:T(8,128)(2,1)S(1)}, bf16[1024,192]{0,1:T(8,128)(2,1)}, u32[]{:S(2)}) copy-start(bf16[1024,192]{0,1:T(8,128)(2,1)} %param.12) | copy-start | bytes 1179652
  55.4 56.6 %copy-start.6 = (f32[1,384]{1,0:T(1,128)S(1)}, f32[1,384]{1,0:T(1,128)}, u32[]{:S(2)}) copy-start(f32[1,384]{1,0:T(1,128)} %v_first.1) | copy-start | bytes 4612
  55.4 56.6 %copy-start.7 = (f32[1,384]{1,0:T(1,128)S(1)}, f32[1,384]{1,0:T(1,128)}, u32[]{:S(2)}) copy-start(f32[1,384]{1,0:T(1,128)} %v_second.1) | copy-start | bytes 4612
  55.5 56.6 %copy-start.8 = (f32[1,192]{1,0:T(1,128)S(1)}, f32[1,192]{1,0:T(1,128)}, u32[]{:S(2)}) copy-start(f32[1,192]{1,0:T(1,128)} %q_first.1) | copy-start | bytes 2308
  55.5 56.6 %copy-start.9 = (f32[1,192]{1,0:T(1,128)S(1)}, f32[1,192]{1,0:T(1,128)}, u32[]{:S(2)}) copy-start(f32[1,192]{1,0:T(1,128)} %q_second.1) | copy-start | bytes 2308
  124.8 21.3 %copy-start.2 = (f32[16,384]{1,0:T(8,128)S(1)}, f32[16,384]{1,0:T(8,128)}, u32[]{:S(2)}) copy-start(f32[16,384]{1,0:T(8,128)} %refs_3_.1) | copy-start | bytes 73732
  124.8 21.3 %copy-start.3 = (f32[16,192]{1,0:T(8,128)S(1)}, f32[16,192]{1,0:T(8,128)}, u32[]{:S(2)}) copy-start(f32[16,192]{1,0:T(8,128)} %refs_4_.1) | copy-start | bytes 36868
  124.8 21.3 %copy-start.4 = (bf16[16,192]{1,0:T(8,128)(2,1)S(1)}, bf16[16,192]{1,0:T(8,128)(2,1)}, u32[]{:S(2)}) copy-start(bf16[16,192]{1,0:T(8,128)(2,1)} %refs_1_.3) | copy-start | bytes 18436
  124.8 21.3 %copy-start.5 = (bf16[16,192]{1,0:T(8,128)(2,1)S(1)}, bf16[16,192]{1,0:T(8,128)(2,1)}, u32[]{:S(2)}) copy-start(bf16[16,192]{1,0:T(8,128)(2,1)} %refs_2_.1) | copy-start | bytes 18436
  124.8 22.3 %slice-start.2 = ((s8[6291456]{0:T(1024)(128)(4,1)}), s8[4194304]{0:T(1024)(128)(4,1)S(1)}, s32[]{:S(2)}) async-start(s8[6291456]{0:T(1024)(128)(4,1)} %bitcast.11), calls=%async_computation.11 | async-start | bytes 8388608
  137.9 9.2 %slice-start.3 = ((s8[6291456]{0:T(1024)(128)(4,1)}), s8[2097152]{0:T(1024)(128)(4,1)S(1)}, s32[]{:S(2)}) async-start(s8[6291456]{0:T(1024)(128)(4,1)} %bitcast.11), calls=%async_computation.12 | async-start | bytes 4194304
Sparse Core Ops, SparseCore 0:
  25.2 73.4 all-gather.1
